TPU v7x, 32 devices: a whole 2x2x4 slice. The times are simulated.
32 devices in a mesh: sp: 8 (over z, x), tp: 4 (over y, core).
Axes of the slice: x: 2, y: 2, z: 4, core: 2. Of those that a mesh axis runs over, the one named last changes fastest.
Arguments:
- query_logits: bfloat16 [4096, 4096], P('sp', 'tp'), may hold values from -6 to 6
- forget_logits: bfloat16 [4096, 4096], P('sp', 'tp'), may hold values from -6 to 6
- value_inputs: bfloat16 [4096, 4096], P('sp', 'tp'), may hold values from -16 to 16
- output_gate_logits: bfloat16 [4096, 4096], P('sp', 'tp'), may hold values from -6 to 6
- forget_floor_gap: float32 [4096], replicated, may hold values from 2.4414063e-05 to 0.1
- surge_log_decay: float32 [32, 4096], P('tp', 'sp'), may hold values from -0.7 to 0
- head_norm_gain: float32 [128], replicated, may hold values from 0.1 to 1.9
- output_matrix: bfloat16 [4096, 4096], P('sp', 'tp'), may hold values from -1.25 to 1.25
- branch_norm_gain: float32 [4096], replicated, may hold values from 0.1 to 1.9
- residual: bfloat16 [4096, 4096], P('sp', 'tp'), may hold values from -6 to 6
Outputs:
- output: bfloat16 [4096, 4096], P('sp', 'tp')
All inputs are finite; a program needn't handle non-finite values.
Results may differ from a plain program's by a relative error of at most 0.005.
Values may be sent and summed in bfloat16 or wider, within the bound.
No kernel may reach another device: no remote copies, remote signals or barrier semaphores. Data moves between devices by JAX's collectives and lax.ppermute only.
A program may use at most 128 MiB of HBM per device.

v0:
```python
import functools

import jax
import jax.numpy as jnp
from jax import lax
from jax.experimental import pallas as pl
from jax.experimental.pallas import tpu as pltpu
from jax.sharding import PartitionSpec as P


HEAD_DIM = 128
SPAN = 128
EXTRA = 8
TILE = 256
ROOM = pltpu.CompilerParams(vmem_limit_bytes=32 * 2**20)
epsilon = 1e-06


f32 = jnp.float32
bf16 = jnp.bfloat16
NN = (((1,), (0,)), ((), ()))
TN = (((0,), (0,)), ((), ()))
NT = (((1,), (1,)), ((), ()))


def dot(a, b, dims=NN):
    return lax.dot_general(a, b, dims, preferred_element_type=f32)


def split2(value):
    high = value.astype(bf16)
    return high, (value - high.astype(f32)).astype(bf16)


def input_gate(forget_logits, gap):
    return gap / (1.0 + jnp.exp(forget_logits.astype(f32)))


def pack_decay(decay):
    first, _ = split2(decay)
    second, third = split2(decay - first.astype(f32))
    rows = [t.astype(f32) for t in (first, second, third)]
    row = lax.broadcasted_iota(jnp.int32, (EXTRA, decay.shape[-1]), 0)
    out = jnp.where(row == 2, rows[2], 0.0)
    return jnp.where(row == 0, rows[0], jnp.where(row == 1, rows[1], out)).astype(bf16)


def unpack(ref, head):
    state = ref[head, :HEAD_DIM, :].astype(f32)
    decay = jnp.sum(ref[head, HEAD_DIM:, :].astype(f32), axis=0, keepdims=True)
    return state, decay


def halves_kernel(matrix_ref, *refs):
    halves, sems = refs[:-1], refs[-1]
    rows = halves[0].shape[0]
    copies = []
    for i, half_ref in enumerate(halves):
        copies.append(pltpu.make_async_copy(matrix_ref.at[pl.ds(i * rows, rows)], half_ref, sems.at[i]))
        copies[-1].start()
    for copy in copies:
        copy.wait()


def states_kernel(first_ref, tp_ref, forget_ref, value_ref, surge_ref, gap_ref, running_ref, packed_ref, column_ref):
    step = pl.program_id(0)
    per = gap_ref.shape[0]
    rows = forget_ref.shape[0]

    @pl.when(step == 0)
    def _():
        column_ref[...] = jnp.transpose(surge_ref[...])

    column = lax.broadcasted_iota(jnp.int32, (SPAN, 2 * SPAN), 1) % SPAN
    lower = (column <= lax.broadcasted_iota(jnp.int32, (SPAN, 2 * SPAN), 0)).astype(bf16)
    surges = column_ref[...]
    lane = lax.broadcasted_iota(jnp.int32, surges.shape, 1)
    for i in range(per):
        cols = slice(i * HEAD_DIM, (i + 1) * HEAD_DIM)
        head = (first_ref[0] + step) * per + i
        gates = input_gate(forget_ref[:, cols], gap_ref[i])
        surge = jnp.sum(jnp.where(lane == head, surges, 0.0), axis=1, keepdims=True)
        high, low = split2(jnp.log1p(-gates) + surge)
        after = jnp.zeros((1, HEAD_DIM), f32)
        keys = []
        for start in reversed(range(0, rows, SPAN)):
            part = slice(start, start + SPAN)
            running = dot(lower, jnp.concatenate([high[part], low[part]], axis=0))
            running_ref[part, cols] = running
            after = after + running[SPAN - 1 :, :]
            keys.append((gates[part] * jnp.exp(after - running)).astype(bf16))
        keys = jnp.concatenate(keys[::-1], axis=0)
        packed_ref[step * per + i, :HEAD_DIM, :] = dot(value_ref[:, cols], keys, TN).astype(bf16)
        packed_ref[step * per + i, HEAD_DIM:, :] = pack_decay(jnp.exp(after))


def local_kernel(first_ref, tp_ref, query_ref, forget_ref, value_ref, running_ref, gap_ref, local_ref, reach_ref):
    rows = query_ref.shape[0]
    row = lax.broadcasted_iota(jnp.int32, (SPAN, SPAN), 0)
    causal = lax.broadcasted_iota(jnp.int32, (SPAN, SPAN), 1) <= row
    for i in range(query_ref.shape[1] // HEAD_DIM):
        cols = slice(i * HEAD_DIM, (i + 1) * HEAD_DIM)
        before = jnp.zeros((1, HEAD_DIM), f32)
        state = None
        for start in range(0, rows, SPAN):
            part = slice(start, start + SPAN)
            logits = query_ref[part, cols].astype(f32)
            queries = logits / (1.0 + jnp.exp(-logits)) * HEAD_DIM**-0.5
            gates = input_gate(forget_ref[part, cols], gap_ref[i])
            values = value_ref[part, cols]
            running = running_ref[part, cols]
            anchor = running[SPAN // 2 - 1 : SPAN // 2, :]
            total = running[SPAN - 1 :, :]
            late = (queries * jnp.exp(running - anchor)).astype(bf16)
            early = (gates * jnp.exp(anchor - running)).astype(bf16)
            scores = jnp.where(causal, dot(late, early, NT), 0.0).astype(bf16)
            out = dot(scores, values)
            faded = queries * jnp.exp(running)
            if state is not None:
                out = out + dot(faded.astype(bf16), state.astype(bf16), NT)
            local_ref[part, cols] = out
            reach_ref[part, cols] = (faded * jnp.exp(before)).astype(bf16)
            if start + SPAN < rows:
                keys = (gates * jnp.exp(total - running)).astype(bf16)
                fresh = dot(values, keys, TN)
                state = fresh if state is None else state * jnp.exp(total) + fresh
                before = before + total


def pair_kernel(odd_ref, own_ref, other_ref, out_ref):
    even = odd_ref[0] == 0
    for head in range(own_ref.shape[0]):
        own, own_decay = unpack(own_ref, head)
        other, other_decay = unpack(other_ref, head)
        mine = jnp.where(even, other_decay, 1.0)
        theirs = jnp.where(even, 1.0, own_decay)
        out_ref[head, :HEAD_DIM, :] = (own * mine + other * theirs).astype(bf16)
        out_ref[head, HEAD_DIM:, :] = pack_decay(own_decay * other_decay)


def unpack_one_of(place, refs, head):
    parts = [unpack(ref, head) for ref in refs]
    if place is None:
        return parts[0]
    return tuple(sum(jnp.where(place == k + 1, part[i], 0.0) for k, part in enumerate(parts)) for i in range(2))


def combine_kernel(*refs, chained):
    place, refs = (refs[0][0] // 2, refs[1:]) if chained else (None, refs)
    later_ref, out_ref = refs[-2:]
    for head in range(later_ref.shape[0]):
        early, early_decay = unpack_one_of(place, refs[:-2], head)
        late, late_decay = unpack(later_ref, head)
        out_ref[head, :HEAD_DIM, :] = (early * late_decay + late).astype(bf16)
        out_ref[head, HEAD_DIM:, :] = pack_decay(early_decay * late_decay)


def carry_kernel(at_ref, *refs, chained):
    own_ref, other_ref, mine_ref, theirs_ref = refs[-4:]
    odd = at_ref[0] % 2 == 1
    place = at_ref[0] // 2 if chained else None
    for head in range(own_ref.shape[0]):
        before, _ = unpack_one_of(place, refs[:-4], head)
        own, own_decay = unpack(own_ref, head)
        other, other_decay = unpack(other_ref, head)
        first = jnp.where(odd, other, own)
        decay = jnp.where(odd, other_decay, own_decay)
        after = before * decay + first
        mine_ref[head] = jnp.where(odd, after, before).astype(bf16)
        theirs_ref[head] = jnp.where(odd, before, after).astype(bf16)


def mix_kernel(first_ref, local_ref, reach_ref, carried_ref, gate_ref, gain_ref, out_ref):
    per = out_ref.shape[1] // HEAD_DIM
    for i in range(per):
        cols = slice(i * HEAD_DIM, (i + 1) * HEAD_DIM)
        carried = carried_ref[pl.program_id(0) * per + i]
        heads_out = local_ref[:, cols] + dot(reach_ref[:, cols], carried, NT)
        mean_sq = jnp.mean(heads_out * heads_out, axis=1, keepdims=True)
        logits = gate_ref[:, cols].astype(f32)
        gates = logits / (1.0 + jnp.exp(-logits))
        mixed = heads_out * lax.rsqrt(mean_sq + epsilon) * gain_ref[...] * gates
        out_ref[:, cols] = mixed.astype(bf16)


def ring_at(place, size):
    return jnp.where(place < size // 2, 2 * place, 2 * (size - 1 - place) + 1)


def place_of(member, size):
    return jnp.where(member % 2 == 0, member // 2, size - 1 - member // 2)


def project_kernel(sp_ref, tp_ref, *refs, offsets, size, n_mixed, kept):
    mixed = refs[:n_mixed]
    chunks = refs[n_mixed : n_mixed + 2 * len(offsets)]
    table = refs[-1]
    group = (sp_ref[0] + 1 - kept) % 2
    at = place_of(sp_ref[0], size)
    half = chunks[0].shape[0]
    for i, piece in enumerate(mixed):
        table[tp_ref[0] ^ i] = piece[...]
    if kept:
        out_ref = refs[-2]
    else:
        partial_ref, out_ref, piece_ref = refs[-4:-1]
        out_ref[...] = partial_ref[...]
        piece_ref[...] = table[ring_at((at + size // 2) % size, size) // 2]

    def add(i, first):
        block = ring_at((at + (offsets[i] + size)) % size, size)

        def product():
            for start in range(0, out_ref.shape[1], TILE):
                cols = slice(start, start + TILE)
                part = dot(table[block // 2, :, :half], chunks[2 * i][:, cols])
                part = part + dot(table[block // 2, :, half:], chunks[2 * i + 1][:, cols])
                out_ref[:, cols] = part if first else out_ref[:, cols] + part

        if first:
            product()
        else:
            pl.when(block % 2 == group)(product)

    for i in range(len(offsets)):
        add(i, kept and i == 0)


def last_kernel(partial_ref, piece_ref, first_ref, second_ref, out_ref, square_ref, lanes_ref):
    half = first_ref.shape[0]
    for start in range(0, out_ref.shape[1], TILE):
        cols = slice(start, start + TILE)
        total = partial_ref[:, cols] + dot(piece_ref[:, :half], first_ref[:, cols])
        rounded = (total + dot(piece_ref[:, half:], second_ref[:, cols])).astype(bf16)
        out_ref[:, cols] = rounded
        wide = rounded.astype(f32)
        squares = wide * wide
        lanes = squares[:, :128]
        for first in range(128, TILE, 128):
            lanes = lanes + squares[:, first : first + 128]
        lanes_ref[...] = lanes if start == 0 else lanes_ref[...] + lanes
    high, low = split2(lanes_ref[...])
    ones = jnp.ones((8, 128), bf16)
    square_ref[...] = (dot(ones, high, NT) + dot(ones, low, NT))[:1]


def norm_kernel(*refs, width, count):
    squares = refs[:-6]
    projected_ref, residual_ref, gain_ref, out_ref, stage_ref, sems = refs[-6:]
    total = squares[0][...]
    for other in squares[1:]:
        total = total + other[...]
    scales = jnp.broadcast_to(lax.rsqrt(total / width + epsilon), (8, total.shape[1]))
    rows = out_ref.shape[0] // count
    copies = []
    for i in range(count):
        part = slice(i * rows, (i + 1) * rows)
        scale = jnp.transpose(scales[:, part])[:, :1]
        branch = projected_ref[part, :].astype(f32) * scale * gain_ref[...]
        stage_ref[part, :] = (residual_ref[part, :].astype(f32) + branch).astype(bf16)
        copies.append(pltpu.make_async_copy(stage_ref.at[pl.ds(i * rows, rows)], out_ref.at[pl.ds(i * rows, rows)], sems.at[i]))
        copies[-1].start()
    for copy in copies:
        copy.wait()


def vmem():
    return pl.BlockSpec(memory_space=pltpu.VMEM)


def smem():
    return pl.BlockSpec(memory_space=pltpu.SMEM)


def resident(array):
    return pltpu.with_memory_space_constraint(array, pltpu.VMEM)


def outside(array):
    return pltpu.with_memory_space_constraint(array, pltpu.HBM)


def small(kernel, scalars, operands, outs, scratch=()):
    return pl.pallas_call(
        kernel,
        out_shape=tuple(pltpu.VMEM(*out) for out in outs),
        in_specs=[smem()] * len(scalars) + [vmem()] * len(operands),
        out_specs=tuple(vmem() for _ in outs),
        scratch_shapes=list(scratch),
        compiler_params=ROOM,
    )(*scalars, *[resident(array) for array in operands])


def call(kernel, scalars, operands, out_shape, grid, in_specs, out_specs, scratch=()):
    spec = pltpu.PrefetchScalarGridSpec(
        num_scalar_prefetch=len(scalars),
        grid=grid,
        in_specs=in_specs,
        out_specs=out_specs,
        scratch_shapes=list(scratch),
    )
    return pl.pallas_call(kernel, grid_spec=spec, out_shape=out_shape, compiler_params=ROOM)(*scalars, *operands)


def is_ringed(sp, tp):
    return sp == 2 * tp and sp <= 8


def ring_gather(halves, axis):
    size = lax.axis_size(axis)
    ring = list(range(0, size, 2)) + list(range(1, size, 2))[::-1]
    forward = [(ring[i], ring[(i + 1) % size]) for i in range(size)]
    backward = [(b, a) for a, b in forward]
    chunks = {0: halves}
    for step in range(1, size // 2):
        chunks[-step], chunks[step] = [None, None], [None, None]
        for part in range(2):
            for sign, pairs, half in ((-1, forward, part), (1, backward, 1 - part)):
                chunks[sign * step][half] = lax.ppermute(chunks[sign * (step - 1)][half], axis, pairs)
    last = size // 2
    chunks[last] = (lax.ppermute(chunks[1 - last][0], axis, forward), lax.ppermute(chunks[last - 1][1], axis, backward))
    return chunks


def swap(array, axis, bit):
    size = lax.axis_size(axis)
    return lax.ppermute(array, axis, [(i, i ^ bit) for i in range(size)])


def shift(array, axis, by):
    size = lax.axis_size(axis)
    return lax.ppermute(array, axis, [(i, i + by) for i in range(size - by)])


def carried_states(given, kept, axis, at):
    size = lax.axis_size(axis)
    other = swap(given, axis, 1)
    (pair,) = small(pair_kernel, (at % 2,), (kept, other), [(kept.shape, bf16)])

    members = size // 2
    chained = members <= 4

    def combine(earlier, later):
        return small(
            functools.partial(combine_kernel, chained=chained),
            (at,) * chained,
            (*earlier, later),
            [(later.shape, bf16)],
        )[0]

    if chained:
        before = []
        for place in range(members - 1):
            sent = combine(before, pair) if before else pair
            pairs = [(2 * place + i, 2 * place + 2 + i) for i in range(2)]
            before.append(lax.ppermute(sent, axis, pairs))
    else:
        earlier, later, reach = shift(pair, axis, 2), None, 2
        while reach < members:
            before = earlier if later is None else combine([earlier], later)
            earlier, later = shift(combine([before], pair), axis, 2 * reach), before
            reach *= 2
        before = [combine([earlier], later)]
    state = ((kept.shape[0], HEAD_DIM, HEAD_DIM), bf16)
    carry = functools.partial(carry_kernel, chained=chained)
    mine, theirs = small(carry, (at,), (*before, kept, other), [state, state])
    return mine, swap(theirs, axis, 1)


def layer(
    query_logits,
    forget_logits,
    value_inputs,
    output_gate_logits,
    forget_floor_gap,
    surge_log_decay,
    head_norm_gain,
    output_matrix,
    branch_norm_gain,
    residual,
):
    rows, head_cols = query_logits.shape
    heads = head_cols // HEAD_DIM
    sp, tp = lax.axis_size("sp"), lax.axis_size("tp")
    sp_at = lax.axis_index("sp").astype(jnp.int32).reshape(1)
    tp_at = lax.axis_index("tp").astype(jnp.int32).reshape(1)
    odd = sp_at % 2
    width = output_matrix.shape[0] * sp
    out_cols = output_matrix.shape[1]
    ringed = is_ringed(sp, tp)

    group = heads // 2
    per = 2
    steps = group // per
    gap = forget_floor_gap.reshape(-1, 1, HEAD_DIM)
    block = pl.BlockSpec((rows, per * HEAD_DIM), lambda s, first, at: (0, first[0] + s))
    own_block = pl.BlockSpec((rows, per * HEAD_DIM), lambda s, first, at: (0, s))
    gap_block = pl.BlockSpec((per, 1, HEAD_DIM), lambda s, first, at: (at[0] * (heads // per) + first[0] + s, 0, 0))
    wide = jax.ShapeDtypeStruct((rows, group * HEAD_DIM), f32)
    narrow = jax.ShapeDtypeStruct((rows, group * HEAD_DIM), bf16)

    def group_states(first, place=lambda array: array):
        return call(
            states_kernel,
            (first, tp_at),
            [place(array) for array in (forget_logits, value_inputs, surge_log_decay, gap)],
            (wide, pltpu.VMEM((group, HEAD_DIM + EXTRA, HEAD_DIM), bf16)),
            (steps,),
            [block, block, pl.BlockSpec((heads, rows), lambda s, first, at: (0, 0)), gap_block],
            (own_block, vmem()),
            [pltpu.VMEM((rows, heads), f32)],
        )

    def group_local(first, running):
        return call(
            local_kernel,
            (first, tp_at),
            (query_logits, forget_logits, value_inputs, running, gap),
            (wide, narrow),
            (steps,),
            [block, block, block, own_block, gap_block],
            (own_block, own_block),
        )

    def group_mix(first, local, reach, carried):
        shared = pl.BlockSpec((rows, per * HEAD_DIM), lambda s, first: (0, s))
        return call(
            mix_kernel,
            (first,),
            (local, reach, resident(carried), output_gate_logits, head_norm_gain.reshape(1, HEAD_DIM)),
            narrow,
            (steps,),
            [
                shared,
                shared,
                vmem(),
                pl.BlockSpec((rows, per * HEAD_DIM), lambda s, first: (0, first[0] + s)),
                pl.BlockSpec((1, HEAD_DIM), lambda s, first: (0, 0)),
            ],
            shared,
        )

    given_first, kept_first = (1 - odd) * steps, odd * steps
    given_running, given = group_states(given_first)
    if ringed:
        halves = pl.pallas_call(
            halves_kernel,
            out_shape=(pltpu.VMEM((output_matrix.shape[0] // 2, out_cols), bf16),) * 2,
            in_specs=[pl.BlockSpec(memory_space=pl.ANY)],
            out_specs=(vmem(), vmem()),
            scratch_shapes=[pltpu.SemaphoreType.DMA((2,))],
            compiler_params=ROOM,
            name="halves",
        )(outside(output_matrix))
        chunks = ring_gather(halves, "sp")
    else:
        whole_weight = lax.all_gather(output_matrix, "sp", axis=0, tiled=True)
    kept_running, kept = group_states(kept_first)
    mine, others = carried_states(given, kept, "sp", sp_at)
    kept_local = group_local(kept_first, kept_running)
    given_local = group_local(given_first, given_running)
    pieces = {0: [group_mix(kept_first, *kept_local, mine), group_mix(given_first, *given_local, others)]}
    bit = tp // 2
    while bit:
        for rel in sorted(pieces):
            pieces[rel ^ bit] = [swap(piece, "tp", bit) for piece in pieces[rel]]
        bit //= 2
    mixed = [piece for rel in range(tp) for piece in pieces[rel]]

    if ringed:
        offsets = [0] + [s * k for k in range(1, sp // 2) for s in (-1, 1)]
        columns = group * HEAD_DIM
        table = [pltpu.VMEM((tp, rows, columns), bf16)]
        partial_sum = ((rows, out_cols), f32)

        def product(kept, outs, *partial):
            places = offsets if kept else offsets[1:]
            return small(
                functools.partial(project_kernel, offsets=places, size=sp, n_mixed=tp, kept=kept),
                (sp_at, tp_at),
                (*mixed[1 - kept :: 2], *[half for off in places for half in chunks[off]], *partial),
                outs,
                table,
            )

        (partial,) = product(1, [partial_sum])
        partial, piece = product(0, [partial_sum, ((rows, columns), bf16)], partial)
        projected, squares = small(
            last_kernel,
            (),
            (partial, piece, *chunks[sp // 2]),
            [((rows, out_cols), bf16), ((1, rows), f32)],
            [pltpu.VMEM((rows, 128), f32)],
        )
    else:
        stacked = jnp.stack(mixed)
        index = jnp.arange(2 * tp, dtype=jnp.int32)
        where = ((index // 2) ^ tp_at[0]) * 2 + (index + odd[0]) % 2
        all_heads = jnp.moveaxis(stacked[where], 0, 1).reshape(rows, width)
        projected = jnp.dot(all_heads, whole_weight, preferred_element_type=f32).astype(bf16)
        branch = lax.optimization_barrier(projected).astype(f32)
        squares = jnp.sum(branch * branch, axis=1)[None]
    others = [swap(squares, "tp", rel) for rel in range(tp - 1, 0, -1)]
    count = 4
    gain = pl.BlockSpec((1, out_cols), lambda n, at: (0, at[0]))
    return call(
        lambda at, *refs: norm_kernel(*refs, width=width, count=count),
        (tp_at,),
        (*[resident(a) for a in (squares, *others, projected, residual)], branch_norm_gain.reshape(1, -1)),
        jax.ShapeDtypeStruct((rows, out_cols), bf16),
        (1,),
        [vmem()] * (tp + 2) + [gain],
        pl.BlockSpec(memory_space=pl.ANY),
        [pltpu.VMEM((rows, out_cols), bf16), pltpu.SemaphoreType.DMA((count,))],
    )


def solution(mesh):
    placed = (
        P("sp", "tp"),
        P("sp", "tp"),
        P("sp", "tp"),
        P("sp", "tp"),
        P(),
        P("tp", "sp"),
        P(),
        P("sp", "tp"),
        P(),
        P("sp", "tp"),
    )
    return jax.shard_map(layer, mesh=mesh, in_specs=placed, out_specs=P("sp", "tp"), check_vma=False)
```

profile of v0, /device:TPU:0, one launch (start us, length us, event | category | flops | bytes accessed | tf_op | source)
XLA Modules:
  0.0 116.0 jit_solution(1903262096906313799)
XLA Ops:
  0.0 1.3 %halves.1 = (bf16[256,1024]{1,0:T(8,128)(2,1)S(1)}, bf16[256,1024]{1,0:T(8,128)(2,1)S(1)}) custom-call(bf16[512,1024]{1,0:T(8,128)(2,1)} %matrix_ref.1), custom_call_target="tpu_custom_call" | custom-call | tf_op jit(solution)/shard_map/halves/pallas_call | solution.py:446
  1.3 3.1 %collective-permute-start.8 = (bf16[256,1024]{1,0:T(8,128)(2,1)S(1)}, bf16[256,1024]{1,0:T(8,128)(2,1)S(1)}, u32[]{:S(2)}, u32[]{:S(2)}) collective-permute-start(bf16[256,1024]{1,0:T(8,128)(2,1)S(1)} %get-tuple-element.27.refs_4_), channel_id=1, source_target_pairs={{0,8},{8,16},{16,24},{24,28},{28,20},{20,12},{12,4},{4,0},{1,9},{9... | collective-permute-start | bytes 1572872 | tf_op jit(solution)/shard_map/ppermute | solution.py:319
  4.4 1.2 %copy-done = bf16[512,1024]{1,0:T(8,128)(2,1)S(1)} copy-done((bf16[512,1024]{1,0:T(8,128)(2,1)S(1)}, bf16[512,1024]{1,0:T(8,128)(2,1)}, u32[]{:S(2)}) %copy-start) | copy-done | bytes 1048600
  5.6 1.2 %copy-done.2 = bf16[512,1024]{1,0:T(8,128)(2,1)S(1)} copy-done((bf16[512,1024]{1,0:T(8,128)(2,1)S(1)}, bf16[512,1024]{1,0:T(8,128)(2,1)}, u32[]{:S(2)}) %copy-start.2) | copy-done | bytes 1048600
  8.3 2.3 %shard_map.100 = (f32[512,512]{1,0:T(8,128)S(1)}, bf16[4,136,128]{2,1,0:T(8,128)(2,1)S(1)}) custom-call(s32[1]{0:T(128)S(6)} %mul.6.first_ref, s32[1]{0:T(128)} %bitcast.tp_ref.at, bf16[512,1024]{1,0:T(8,128)(2,1)S(1)} %copy-done, bf16[512,1024]{1,0:T(8,128)(2,1)S(1)} %copy-done.2, f32[8,512]{1,0:T(8,128)S(1)} %copy-done.9, f32[32,1,128]{2,1,0:T(1,128)S(1)} %bitcast.5), custom_call_target="tpu_custom_call" | custom-call | tf_op jit(solution)/shard_map/pallas_call | solution.py:302
  10.7 2.3 %shard_map.102 = (f32[512,512]{1,0:T(8,128)S(1)}, bf16[4,136,128]{2,1,0:T(8,128)(2,1)S(1)}) custom-call(s32[1]{0:T(128)S(6)} %mul.7.first_ref, s32[1]{0:T(128)} %bitcast.tp_ref.at, bf16[512,1024]{1,0:T(8,128)(2,1)S(1)} %copy-done.1, bf16[512,1024]{1,0:T(8,128)(2,1)S(1)} %copy-done.3, f32[8,512]{1,0:T(8,128)S(1)} %copy-done.9, f32[32,1,128]{2,1,0:T(1,128)S(1)} %bitcast.6), custom_call_target="tpu_custom_call" | custom-call | tf_op jit(solution)/shard_map/pallas_call | solution.py:302
  13.0 6.3 %collective-permute-done.other_ref.refs_4_ = bf16[4,136,128]{2,1,0:T(8,128)(2,1)S(1)} collective-permute-done((bf16[4,136,128]{2,1,0:T(8,128)(2,1)S(1)}, bf16[4,136,128]{2,1,0:T(8,128)(2,1)S(1)}, u32[]{:S(2)}, u32[]{:S(2)}) %collective-permute-start) | collective-permute-done | bytes 139296 | tf_op jit(solution)/shard_map/ppermute | solution.py:327
  19.3 1.3 %collective-permute-start.1 = (bf16[4,136,128]{2,1,0:T(8,128)(2,1)S(1)}, bf16[4,136,128]{2,1,0:T(8,128)(2,1)S(1)}, u32[]{:S(2)}, u32[]{:S(2)}) collective-permute-start(bf16[4,136,128]{2,1,0:T(8,128)(2,1)S(1)} %shard_map.103.refs_2_.refs_3_), channel_id=1, source_target_pairs={{0,8},{4,12},{1,9},{5,13},{2,10},{6,14},{3,11},{7,15}} | collective-permute-start | bytes 417800 | tf_op jit(solution)/shard_map/ppermute | solution.py:356
  20.7 2.0 %collective-permute-start.9 = (bf16[256,1024]{1,0:T(8,128)(2,1)S(1)}, bf16[256,1024]{1,0:T(8,128)(2,1)S(1)}, u32[]{:S(2)}, u32[]{:S(2)}) collective-permute-start(bf16[256,1024]{1,0:T(8,128)(2,1)S(1)} %get-tuple-element.28.refs_5_), channel_id=1, source_target_pairs={{0,8},{8,16},{16,24},{24,28},{28,20},{20,12},{12,4},{4,0},{1,9},{9... | collective-permute-start | bytes 1572872 | tf_op jit(solution)/shard_map/ppermute | solution.py:319
  22.8 2.0 %collective-permute-start.12 = (bf16[256,1024]{1,0:T(8,128)(2,1)S(1)}, bf16[256,1024]{1,0:T(8,128)(2,1)S(1)}, u32[]{:S(2)}, u32[]{:S(2)}) collective-permute-start(bf16[256,1024]{1,0:T(8,128)(2,1)S(1)} %collective-permute-done.8.refs_6_.refs_4_), channel_id=1, source_target_pairs={{0,8},{8,16},{16,24},{24,28},{28,20},{20,12},{12,4},{4,0},{1,9},{9... | collective-permute-start | bytes 1572872 | tf_op jit(solution)/shard_map/ppermute | solution.py:319
  26.6 2.6 %shard_map.108 = (f32[512,512]{1,0:T(8,128)S(1)}, bf16[512,512]{1,0:T(8,128)(2,1)S(1)}) custom-call(s32[1]{0:T(128)S(6)} %mul.7.first_ref, s32[1]{0:T(128)} %bitcast.tp_ref.at, bf16[512,1024]{1,0:T(8,128)(2,1)S(1)} %copy-done.4, bf16[512,1024]{1,0:T(8,128)(2,1)S(1)} %copy-done.1, bf16[512,1024]{1,0:T(8,128)(2,1)S(1)} %copy-done.3, ...), custom_call_target="tpu_custom_call" | custom-call | tf_op jit(solution)/shard_map/pallas_call | solution.py:302
  29.2 6.2 %collective-permute-done.11.refs_9_.refs_7_ = bf16[256,1024]{1,0:T(8,128)(2,1)S(1)} collective-permute-done((bf16[256,1024]{1,0:T(8,128)(2,1)S(1)}, bf16[256,1024]{1,0:T(8,128)(2,1)S(1)}, u32[]{:S(2)}, u32[]{:S(2)}) %collective-permute-start.11) | collective-permute-done | bytes 524320 | tf_op jit(solution)/shard_map/ppermute | solution.py:319
  35.9 15.5 %collective-permute-start.13 = (bf16[256,1024]{1,0:T(8,128)(2,1)S(1)}, bf16[256,1024]{1,0:T(8,128)(2,1)S(1)}, u32[]{:S(2)}, u32[]{:S(2)}) collective-permute-start(bf16[256,1024]{1,0:T(8,128)(2,1)S(1)} %collective-permute-done.9.refs_7_.refs_5_), channel_id=1, source_target_pairs={{0,8},{8,16},{16,24},{24,28},{28,20},{20,12},{12,4},{4,0},{1,9},{9... | collective-permute-start | bytes 1572872 | tf_op jit(solution)/shard_map/ppermute | solution.py:319
  51.4 1.9 %collective-permute-start.14 = (bf16[256,1024]{1,0:T(8,128)(2,1)S(1)}, bf16[256,1024]{1,0:T(8,128)(2,1)S(1)}, u32[]{:S(2)}, u32[]{:S(2)}) collective-permute-start(bf16[256,1024]{1,0:T(8,128)(2,1)S(1)} %collective-permute-done.10.refs_8_.refs_6_), channel_id=1, source_target_pairs={{8,0},{16,8},{24,16},{28,24},{20,28},{12,20},{4,12},{0,4},{9,1},{1... | collective-permute-start | bytes 1572872 | tf_op jit(solution)/shard_map/ppermute | solution.py:319
  53.3 1.2 shard_map.109.refs_0_
  54.5 1.6 %collective-permute-start.21 = (bf16[512,512]{1,0:T(8,128)(2,1)S(1)}, bf16[512,512]{1,0:T(8,128)(2,1)S(1)}, u32[]{:S(2)}, u32[]{:S(2)}) collective-permute-start(bf16[512,512]{1,0:T(8,128)(2,1)S(1)} %shard_map.109.refs_0_), channel_id=1, source_target_pairs={{0,2},{1,3},{2,0},{3,1},{4,6},{5,7},{6,4},{7,5},{8,10},{9,11},{10,... | collective-permute-start | bytes 1572872 | tf_op jit(solution)/shard_map/ppermute | solution.py:327
  56.1 2.6 %shard_map.101 = (f32[512,512]{1,0:T(8,128)S(1)}, bf16[512,512]{1,0:T(8,128)(2,1)S(1)}) custom-call(s32[1]{0:T(128)S(6)} %mul.6.first_ref, s32[1]{0:T(128)} %bitcast.tp_ref.at, bf16[512,1024]{1,0:T(8,128)(2,1)S(1)} %copy-done.4, bf16[512,1024]{1,0:T(8,128)(2,1)S(1)} %copy-done.1, bf16[512,1024]{1,0:T(8,128)(2,1)S(1)} %copy-done.3, ...), custom_call_target="tpu_custom_call" | custom-call | tf_op jit(solution)/shard_map/pallas_call | solution.py:302
  58.7 1.2 %shard_map.107.refs_0_ = bf16[512,512]{1,0:T(8,128)(2,1)S(1)} custom-call(s32[1]{0:T(128)S(6)} %mul.6.first_ref, f32[512,512]{1,0:T(8,128)S(1)} %get-tuple-element.22.local_ref, bf16[512,512]{1,0:T(8,128)(2,1)S(1)} %get-tuple-element.23.reach_ref, bf16[4,128,128]{2,1,0:T(8,128)(2,1)S(1)} %collective-permute-done.4.carried_ref, ...), custom_call_target="tpu_custom_call" | custom-call | tf_op jit(solution)/shard_map/pallas_call | solution.py:302
  59.9 4.2 %collective-permute-done.15.refs_13_.refs_11_ = bf16[256,1024]{1,0:T(8,128)(2,1)S(1)} collective-permute-done((bf16[256,1024]{1,0:T(8,128)(2,1)S(1)}, bf16[256,1024]{1,0:T(8,128)(2,1)S(1)}, u32[]{:S(2)}, u32[]{:S(2)}) %collective-permute-start.15) | collective-permute-done | bytes 524320 | tf_op jit(solution)/shard_map/ppermute | solution.py:319
  64.1 1.5 %collective-permute-start.6 = (bf16[512,512]{1,0:T(8,128)(2,1)S(1)}, bf16[512,512]{1,0:T(8,128)(2,1)S(1)}, u32[]{:S(2)}, u32[]{:S(2)}) collective-permute-start(bf16[512,512]{1,0:T(8,128)(2,1)S(1)} %shard_map.107.refs_0_), channel_id=1, source_target_pairs={{0,2},{1,3},{2,0},{3,1},{4,6},{5,7},{6,4},{7,5},{8,10},{9,11},{10,... | collective-permute-start | bytes 1572872 | tf_op jit(solution)/shard_map/ppermute | solution.py:327
  65.6 5.7 %collective-permute-start.16 = (bf16[256,1024]{1,0:T(8,128)(2,1)S(1)}, bf16[256,1024]{1,0:T(8,128)(2,1)S(1)}, u32[]{:S(2)}, u32[]{:S(2)}) collective-permute-start(bf16[256,1024]{1,0:T(8,128)(2,1)S(1)} %collective-permute-done.12.refs_10_.refs_8_), channel_id=1, source_target_pairs={{0,8},{8,16},{16,24},{24,28},{28,20},{20,12},{12,4},{4,0},{1,9},{9... | collective-permute-start | bytes 1572872 | tf_op jit(solution)/shard_map/ppermute | solution.py:319
  71.2 1.8 %collective-permute-done.14.refs_12_.refs_10_ = bf16[256,1024]{1,0:T(8,128)(2,1)S(1)} collective-permute-done((bf16[256,1024]{1,0:T(8,128)(2,1)S(1)}, bf16[256,1024]{1,0:T(8,128)(2,1)S(1)}, u32[]{:S(2)}, u32[]{:S(2)}) %collective-permute-start.14) | collective-permute-done | bytes 524320 | tf_op jit(solution)/shard_map/ppermute | solution.py:319
  74.0 4.2 %collective-permute-start.17 = (bf16[256,1024]{1,0:T(8,128)(2,1)S(1)}, bf16[256,1024]{1,0:T(8,128)(2,1)S(1)}, u32[]{:S(2)}, u32[]{:S(2)}) collective-permute-start(bf16[256,1024]{1,0:T(8,128)(2,1)S(1)} %collective-permute-done.13.refs_11_.refs_9_), channel_id=1, source_target_pairs={{0,8},{8,16},{16,24},{24,28},{28,20},{20,12},{12,4},{4,0},{1,9},{9... | collective-permute-start | bytes 1572872 | tf_op jit(solution)/shard_map/ppermute | solution.py:319
  78.1 1.7 %collective-permute-start.18 = (bf16[256,1024]{1,0:T(8,128)(2,1)S(1)}, bf16[256,1024]{1,0:T(8,128)(2,1)S(1)}, u32[]{:S(2)}, u32[]{:S(2)}) collective-permute-start(bf16[256,1024]{1,0:T(8,128)(2,1)S(1)} %collective-permute-done.14.refs_12_.refs_10_), channel_id=1, source_target_pairs={{8,0},{16,8},{24,16},{28,24},{20,28},{12,20},{4,12},{0,4},{9,1},{1... | collective-permute-start | bytes 1572872 | tf_op jit(solution)/shard_map/ppermute | solution.py:319
  80.6 10.3 %collective-permute-done.19.refs_17_.refs_15_ = bf16[256,1024]{1,0:T(8,128)(2,1)S(1)} collective-permute-done((bf16[256,1024]{1,0:T(8,128)(2,1)S(1)}, bf16[256,1024]{1,0:T(8,128)(2,1)S(1)}, u32[]{:S(2)}, u32[]{:S(2)}) %collective-permute-start.19) | collective-permute-done | bytes 524320 | tf_op jit(solution)/shard_map/ppermute | solution.py:319
  90.9 2.1 %collective-permute-start.23 = (bf16[256,1024]{1,0:T(8,128)(2,1)S(1)}, bf16[256,1024]{1,0:T(8,128)(2,1)S(1)}, u32[]{:S(2)}, u32[]{:S(2)}) collective-permute-start(bf16[256,1024]{1,0:T(8,128)(2,1)S(1)} %collective-permute-done.16.refs_14_.refs_12_), channel_id=1, source_target_pairs={{0,8},{8,16},{16,24},{24,28},{28,20},{20,12},{12,4},{4,0},{1,9},{9... | collective-permute-start | bytes 1572872 | tf_op jit(solution)/shard_map/ppermute | solution.py:321
  93.1 6.4 %collective-permute-done.18.refs_16_.refs_14_ = bf16[256,1024]{1,0:T(8,128)(2,1)S(1)} collective-permute-done((bf16[256,1024]{1,0:T(8,128)(2,1)S(1)}, bf16[256,1024]{1,0:T(8,128)(2,1)S(1)}, u32[]{:S(2)}, u32[]{:S(2)}) %collective-permute-start.18) | collective-permute-done | bytes 524320 | tf_op jit(solution)/shard_map/ppermute | solution.py:319
  99.4 3.0 %shard_map.110.refs_16_ = f32[512,1024]{1,0:T(8,128)S(1)} custom-call(s32[1]{0:T(128)} %bitcast.1.refs_0_.at_ref.sp_ref, s32[1]{0:T(128)} %bitcast.tp_ref.at, bf16[512,512]{1,0:T(8,128)(2,1)S(1)} %shard_map.109.refs_0_, bf16[512,512]{1,0:T(8,128)(2,1)S(1)} %collective-permute-done.20.refs_1_, bf16[512,512]{1,0:T(8,128)(2,1)S(1)} %collective-permute-done.21.refs_2_, ...), custom_call_target="tpu_custom_call" | custom-call | tf_op jit(solution)/shard_map/pallas_call | solution.py:284
  102.5 2.7 %shard_map.111 = (f32[512,1024]{1,0:T(8,128)S(1)}, bf16[512,512]{1,0:T(8,128)(2,1)S(1)}) custom-call(s32[1]{0:T(128)} %bitcast.1.refs_0_.at_ref.sp_ref, s32[1]{0:T(128)} %bitcast.tp_ref.at, bf16[512,512]{1,0:T(8,128)(2,1)S(1)} %shard_map.107.refs_0_, bf16[512,512]{1,0:T(8,128)(2,1)S(1)} %collective-permute-done.5.refs_1_, ...), custom_call_target="tpu_custom_call" | custom-call | tf_op jit(solution)/shard_map/pallas_call | solution.py:284
  105.3 4.7 %collective-permute-done.24.second_ref = bf16[256,1024]{1,0:T(8,128)(2,1)S(1)} collective-permute-done((bf16[256,1024]{1,0:T(8,128)(2,1)S(1)}, bf16[256,1024]{1,0:T(8,128)(2,1)S(1)}, u32[]{:S(2)}, u32[]{:S(2)}) %collective-permute-start.24) | collective-permute-done | bytes 524320 | tf_op jit(solution)/shard_map/ppermute | solution.py:321
  112.8 1.1 collective-permute-done.25.refs_1_
  114.5 1.3 %shard_map.113 = bf16[512,1024]{1,0:T(8,128)(2,1)} custom-call(s32[1]{0:T(128)} %bitcast.tp_ref.at, f32[1,512]{1,0:T(1,128)S(1)} %get-tuple-element.35.refs_0_, f32[1,512]{1,0:T(1,128)S(1)} %collective-permute-done.25.refs_1_, f32[1,512]{1,0:T(1,128)S(1)} %collective-permute-done.26.refs_2_, f32[1,512]{1,0:T(1,128)S(1)} %collective-permute-done.27.refs_3_, ...), custom_call_target="tpu_custom_call" | custom-call | tf_op jit(solution)/shard_map/pallas_call | solution.py:302
  (63 shorter events, 9.2 us)
Async XLA Ops:
  0.0 10.7 %copy-start.1 = (bf16[512,1024]{1,0:T(8,128)(2,1)S(1)}, bf16[512,1024]{1,0:T(8,128)(2,1)}, u32[]{:S(2)}) copy-start(bf16[512,1024]{1,0:T(8,128)(2,1)} %forget_ref.7) | copy-start | bytes 3145732
  1.3 21.5 %collective-permute-start.8 = (bf16[256,1024]{1,0:T(8,128)(2,1)S(1)}, bf16[256,1024]{1,0:T(8,128)(2,1)S(1)}, u32[]{:S(2)}, u32[]{:S(2)}) collective-permute-start(bf16[256,1024]{1,0:T(8,128)(2,1)S(1)} %get-tuple-element.27.refs_4_), channel_id=1, source_target_pairs={{0,8},{8,16},{16,24},{24,28},{28,20},{20,12},{12,4},{4,0},{1,9},{9... | collective-permute-start | bytes 1572872 | tf_op jit(solution)/shard_map/ppermute | solution.py:319
  10.6 8.7 %collective-permute-start = (bf16[4,136,128]{2,1,0:T(8,128)(2,1)S(1)}, bf16[4,136,128]{2,1,0:T(8,128)(2,1)S(1)}, u32[]{:S(2)}, u32[]{:S(2)}) collective-permute-start(bf16[4,136,128]{2,1,0:T(8,128)(2,1)S(1)} %get-tuple-element.25), channel_id=1, source_target_pairs={{0,4},{4,0},{8,12},{12,8},{16,20},{20,16},{24,28},{28,24},{1,5},{5... | collective-permute-start | bytes 417800 | tf_op jit(solution)/shard_map/ppermute | solution.py:327
  10.7 15.9 %copy-start.4 = (bf16[512,1024]{1,0:T(8,128)(2,1)S(1)}, bf16[512,1024]{1,0:T(8,128)(2,1)}, u32[]{:S(2)}) copy-start(bf16[512,1024]{1,0:T(8,128)(2,1)} %query_ref.3) | copy-start | bytes 3145732
  19.3 5.4 %collective-permute-start.1 = (bf16[4,136,128]{2,1,0:T(8,128)(2,1)S(1)}, bf16[4,136,128]{2,1,0:T(8,128)(2,1)S(1)}, u32[]{:S(2)}, u32[]{:S(2)}) collective-permute-start(bf16[4,136,128]{2,1,0:T(8,128)(2,1)S(1)} %shard_map.103.refs_2_.refs_3_), channel_id=1, source_target_pairs={{0,8},{4,12},{1,9},{5,13},{2,10},{6,14},{3,11},{7,15}} | collective-permute-start | bytes 417800 | tf_op jit(solution)/shard_map/ppermute | solution.py:356
  20.6 14.8 %collective-permute-start.11 = (bf16[256,1024]{1,0:T(8,128)(2,1)S(1)}, bf16[256,1024]{1,0:T(8,128)(2,1)S(1)}, u32[]{:S(2)}, u32[]{:S(2)}) collective-permute-start(bf16[256,1024]{1,0:T(8,128)(2,1)S(1)} %get-tuple-element.28.refs_5_), channel_id=1, source_target_pairs={{8,0},{16,8},{24,16},{28,24},{20,28},{12,20},{4,12},{0,4},{9,1},{1... | collective-permute-start | bytes 1572872 | tf_op jit(solution)/shard_map/ppermute | solution.py:319
  20.7 15.2 %collective-permute-start.9 = (bf16[256,1024]{1,0:T(8,128)(2,1)S(1)}, bf16[256,1024]{1,0:T(8,128)(2,1)S(1)}, u32[]{:S(2)}, u32[]{:S(2)}) collective-permute-start(bf16[256,1024]{1,0:T(8,128)(2,1)S(1)} %get-tuple-element.28.refs_5_), channel_id=1, source_target_pairs={{0,8},{8,16},{16,24},{24,28},{28,20},{20,12},{12,4},{4,0},{1,9},{9... | collective-permute-start | bytes 1572872 | tf_op jit(solution)/shard_map/ppermute | solution.py:319
  22.7 28.7 %collective-permute-start.10 = (bf16[256,1024]{1,0:T(8,128)(2,1)S(1)}, bf16[256,1024]{1,0:T(8,128)(2,1)S(1)}, u32[]{:S(2)}, u32[]{:S(2)}) collective-permute-start(bf16[256,1024]{1,0:T(8,128)(2,1)S(1)} %get-tuple-element.27.refs_4_), channel_id=1, source_target_pairs={{8,0},{16,8},{24,16},{28,24},{20,28},{12,20},{4,12},{0,4},{9,1},{1... | collective-permute-start | bytes 1572872 | tf_op jit(solution)/shard_map/ppermute | solution.py:319
  22.8 33.3 %collective-permute-start.12 = (bf16[256,1024]{1,0:T(8,128)(2,1)S(1)}, bf16[256,1024]{1,0:T(8,128)(2,1)S(1)}, u32[]{:S(2)}, u32[]{:S(2)}) collective-permute-start(bf16[256,1024]{1,0:T(8,128)(2,1)S(1)} %collective-permute-done.8.refs_6_.refs_4_), channel_id=1, source_target_pairs={{0,8},{8,16},{16,24},{24,28},{28,20},{20,12},{12,4},{4,0},{1,9},{9... | collective-permute-start | bytes 1572872 | tf_op jit(solution)/shard_map/ppermute | solution.py:319
  24.8 0.7 collective-permute-start.2
  25.6 0.7 collective-permute-start.3
  26.5 28.0 %collective-permute-start.4 = (bf16[4,128,128]{2,1,0:T(8,128)(2,1)S(1)}, bf16[4,128,128]{2,1,0:T(8,128)(2,1)S(1)}, u32[]{:S(2)}, u32[]{:S(2)}) collective-permute-start(bf16[4,128,128]{2,1,0:T(8,128)(2,1)S(1)} %get-tuple-element.26), channel_id=1, source_target_pairs={{0,4},{4,0},{8,12},{12,8},{16,20},{20,16},{24,28},{28,24},{1,5},{5... | collective-permute-start | bytes 393224 | tf_op jit(solution)/shard_map/ppermute | solution.py:327
  26.6 26.7 %copy-start.5 = (bf16[512,1024]{1,0:T(8,128)(2,1)S(1)}, bf16[512,1024]{1,0:T(8,128)(2,1)}, u32[]{:S(2)}) copy-start(bf16[512,1024]{1,0:T(8,128)(2,1)} %gate_ref.3) | copy-start | bytes 3145732
  26.6 26.7 %copy-start.11 = (f32[128]{0:T(128)S(1)}, f32[128]{0:T(128)}, u32[]{:S(2)}) copy-start(f32[128]{0:T(128)} %param.16) | copy-start | bytes 1540
  35.5 28.6 %collective-permute-start.15 = (bf16[256,1024]{1,0:T(8,128)(2,1)S(1)}, bf16[256,1024]{1,0:T(8,128)(2,1)S(1)}, u32[]{:S(2)}, u32[]{:S(2)}) collective-permute-start(bf16[256,1024]{1,0:T(8,128)(2,1)S(1)} %collective-permute-done.11.refs_9_.refs_7_), channel_id=1, source_target_pairs={{8,0},{16,8},{24,16},{28,24},{20,28},{12,20},{4,12},{0,4},{9,1},{1... | collective-permute-start | bytes 1572872 | tf_op jit(solution)/shard_map/ppermute | solution.py:319
  35.9 29.7 %collective-permute-start.13 = (bf16[256,1024]{1,0:T(8,128)(2,1)S(1)}, bf16[256,1024]{1,0:T(8,128)(2,1)S(1)}, u32[]{:S(2)}, u32[]{:S(2)}) collective-permute-start(bf16[256,1024]{1,0:T(8,128)(2,1)S(1)} %collective-permute-done.9.refs_7_.refs_5_), channel_id=1, source_target_pairs={{0,8},{8,16},{16,24},{24,28},{28,20},{20,12},{12,4},{4,0},{1,9},{9... | collective-permute-start | bytes 1572872 | tf_op jit(solution)/shard_map/ppermute | solution.py:319
  51.4 21.6 %collective-permute-start.14 = (bf16[256,1024]{1,0:T(8,128)(2,1)S(1)}, bf16[256,1024]{1,0:T(8,128)(2,1)S(1)}, u32[]{:S(2)}, u32[]{:S(2)}) collective-permute-start(bf16[256,1024]{1,0:T(8,128)(2,1)S(1)} %collective-permute-done.10.refs_8_.refs_6_), channel_id=1, source_target_pairs={{8,0},{16,8},{24,16},{28,24},{20,28},{12,20},{4,12},{0,4},{9,1},{1... | collective-permute-start | bytes 1572872 | tf_op jit(solution)/shard_map/ppermute | solution.py:319
  54.5 19.5 %collective-permute-start.21 = (bf16[512,512]{1,0:T(8,128)(2,1)S(1)}, bf16[512,512]{1,0:T(8,128)(2,1)S(1)}, u32[]{:S(2)}, u32[]{:S(2)}) collective-permute-start(bf16[512,512]{1,0:T(8,128)(2,1)S(1)} %shard_map.109.refs_0_), channel_id=1, source_target_pairs={{0,2},{1,3},{2,0},{3,1},{4,6},{5,7},{6,4},{7,5},{8,10},{9,11},{10,... | collective-permute-start | bytes 1572872 | tf_op jit(solution)/shard_map/ppermute | solution.py:327
  56.1 22.1 %collective-permute-start.20 = (bf16[512,512]{1,0:T(8,128)(2,1)S(1)}, bf16[512,512]{1,0:T(8,128)(2,1)S(1)}, u32[]{:S(2)}, u32[]{:S(2)}) collective-permute-start(bf16[512,512]{1,0:T(8,128)(2,1)S(1)} %shard_map.109.refs_0_), channel_id=1, source_target_pairs={{0,1},{1,0},{2,3},{3,2},{4,5},{5,4},{6,7},{7,6},{8,9},{9,8},{10,11... | collective-permute-start | bytes 1572872 | tf_op jit(solution)/shard_map/ppermute | solution.py:327
  64.1 15.8 %collective-permute-start.6 = (bf16[512,512]{1,0:T(8,128)(2,1)S(1)}, bf16[512,512]{1,0:T(8,128)(2,1)S(1)}, u32[]{:S(2)}, u32[]{:S(2)}) collective-permute-start(bf16[512,512]{1,0:T(8,128)(2,1)S(1)} %shard_map.107.refs_0_), channel_id=1, source_target_pairs={{0,2},{1,3},{2,0},{3,1},{4,6},{5,7},{6,4},{7,5},{8,10},{9,11},{10,... | collective-permute-start | bytes 1572872 | tf_op jit(solution)/shard_map/ppermute | solution.py:327
  65.6 15.0 %collective-permute-start.16 = (bf16[256,1024]{1,0:T(8,128)(2,1)S(1)}, bf16[256,1024]{1,0:T(8,128)(2,1)S(1)}, u32[]{:S(2)}, u32[]{:S(2)}) collective-permute-start(bf16[256,1024]{1,0:T(8,128)(2,1)S(1)} %collective-permute-done.12.refs_10_.refs_8_), channel_id=1, source_target_pairs={{0,8},{8,16},{16,24},{24,28},{28,20},{20,12},{12,4},{4,0},{1,9},{9... | collective-permute-start | bytes 1572872 | tf_op jit(solution)/shard_map/ppermute | solution.py:319
  73.0 17.9 %collective-permute-start.19 = (bf16[256,1024]{1,0:T(8,128)(2,1)S(1)}, bf16[256,1024]{1,0:T(8,128)(2,1)S(1)}, u32[]{:S(2)}, u32[]{:S(2)}) collective-permute-start(bf16[256,1024]{1,0:T(8,128)(2,1)S(1)} %collective-permute-done.15.refs_13_.refs_11_), channel_id=1, source_target_pairs={{8,0},{16,8},{24,16},{28,24},{20,28},{12,20},{4,12},{0,4},{9,1},{1... | collective-permute-start | bytes 1572872 | tf_op jit(solution)/shard_map/ppermute | solution.py:319
  74.0 16.9 %collective-permute-start.17 = (bf16[256,1024]{1,0:T(8,128)(2,1)S(1)}, bf16[256,1024]{1,0:T(8,128)(2,1)S(1)}, u32[]{:S(2)}, u32[]{:S(2)}) collective-permute-start(bf16[256,1024]{1,0:T(8,128)(2,1)S(1)} %collective-permute-done.13.refs_11_.refs_9_), channel_id=1, source_target_pairs={{0,8},{8,16},{16,24},{24,28},{28,20},{20,12},{12,4},{4,0},{1,9},{9... | collective-permute-start | bytes 1572872 | tf_op jit(solution)/shard_map/ppermute | solution.py:319
  78.1 21.3 %collective-permute-start.18 = (bf16[256,1024]{1,0:T(8,128)(2,1)S(1)}, bf16[256,1024]{1,0:T(8,128)(2,1)S(1)}, u32[]{:S(2)}, u32[]{:S(2)}) collective-permute-start(bf16[256,1024]{1,0:T(8,128)(2,1)S(1)} %collective-permute-done.14.refs_12_.refs_10_), channel_id=1, source_target_pairs={{8,0},{16,8},{24,16},{28,24},{20,28},{12,20},{4,12},{0,4},{9,1},{1... | collective-permute-start | bytes 1572872 | tf_op jit(solution)/shard_map/ppermute | solution.py:319
  79.8 22.7 %collective-permute-start.5 = (bf16[512,512]{1,0:T(8,128)(2,1)S(1)}, bf16[512,512]{1,0:T(8,128)(2,1)S(1)}, u32[]{:S(2)}, u32[]{:S(2)}) collective-permute-start(bf16[512,512]{1,0:T(8,128)(2,1)S(1)} %shard_map.107.refs_0_), channel_id=1, source_target_pairs={{0,1},{1,0},{2,3},{3,2},{4,5},{5,4},{6,7},{7,6},{8,9},{9,8},{10,11... | collective-permute-start | bytes 1572872 | tf_op jit(solution)/shard_map/ppermute | solution.py:327
  80.6 18.9 %collective-permute-start.22 = (bf16[512,512]{1,0:T(8,128)(2,1)S(1)}, bf16[512,512]{1,0:T(8,128)(2,1)S(1)}, u32[]{:S(2)}, u32[]{:S(2)}) collective-permute-start(bf16[512,512]{1,0:T(8,128)(2,1)S(1)} %collective-permute-done.21.refs_2_), channel_id=1, source_target_pairs={{0,1},{1,0},{2,3},{3,2},{4,5},{5,4},{6,7},{7,6},{8,9},{9,8},{10,11... | collective-permute-start | bytes 1572872 | tf_op jit(solution)/shard_map/ppermute | solution.py:327
  90.9 11.6 %collective-permute-start.7 = (bf16[512,512]{1,0:T(8,128)(2,1)S(1)}, bf16[512,512]{1,0:T(8,128)(2,1)S(1)}, u32[]{:S(2)}, u32[]{:S(2)}) collective-permute-start(bf16[512,512]{1,0:T(8,128)(2,1)S(1)} %collective-permute-done.6.refs_2_), channel_id=1, source_target_pairs={{0,1},{1,0},{2,3},{3,2},{4,5},{5,4},{6,7},{7,6},{8,9},{9,8},{10,11... | collective-permute-start | bytes 1572872 | tf_op jit(solution)/shard_map/ppermute | solution.py:327
  90.9 14.3 %collective-permute-start.23 = (bf16[256,1024]{1,0:T(8,128)(2,1)S(1)}, bf16[256,1024]{1,0:T(8,128)(2,1)S(1)}, u32[]{:S(2)}, u32[]{:S(2)}) collective-permute-start(bf16[256,1024]{1,0:T(8,128)(2,1)S(1)} %collective-permute-done.16.refs_14_.refs_12_), channel_id=1, source_target_pairs={{0,8},{8,16},{16,24},{24,28},{28,20},{20,12},{12,4},{4,0},{1,9},{9... | collective-permute-start | bytes 1572872 | tf_op jit(solution)/shard_map/ppermute | solution.py:321
  99.4 10.5 %collective-permute-start.24 = (bf16[256,1024]{1,0:T(8,128)(2,1)S(1)}, bf16[256,1024]{1,0:T(8,128)(2,1)S(1)}, u32[]{:S(2)}, u32[]{:S(2)}) collective-permute-start(bf16[256,1024]{1,0:T(8,128)(2,1)S(1)} %collective-permute-done.19.refs_17_.refs_15_), channel_id=1, source_target_pairs={{8,0},{16,8},{24,16},{28,24},{20,28},{12,20},{4,12},{0,4},{9,1},{1... | collective-permute-start | bytes 1572872 | tf_op jit(solution)/shard_map/ppermute | solution.py:321
  110.9 3.0 %collective-permute-start.25 = (f32[1,512]{1,0:T(1,128)S(1)}, f32[1,512]{1,0:T(1,128)S(1)}, u32[]{:S(2)}, u32[]{:S(2)}) collective-permute-start(f32[1,512]{1,0:T(1,128)S(1)} %get-tuple-element.35.refs_0_), channel_id=1, source_target_pairs={{0,3},{1,2},{2,1},{3,0},{4,7},{5,6},{6,5},{7,4},{8,11},{9,10},{10,... | collective-permute-start | bytes 6152 | tf_op jit(solution)/shard_map/ppermute | solution.py:327
  110.9 3.6 %collective-permute-start.26 = (f32[1,512]{1,0:T(1,128)S(1)}, f32[1,512]{1,0:T(1,128)S(1)}, u32[]{:S(2)}, u32[]{:S(2)}) collective-permute-start(f32[1,512]{1,0:T(1,128)S(1)} %get-tuple-element.35.refs_0_), channel_id=1, source_target_pairs={{0,2},{1,3},{2,0},{3,1},{4,6},{5,7},{6,4},{7,5},{8,10},{9,11},{10,... | collective-permute-start | bytes 6152 | tf_op jit(solution)/shard_map/ppermute | solution.py:327
  111.9 2.7 %collective-permute-start.27 = (f32[1,512]{1,0:T(1,128)S(1)}, f32[1,512]{1,0:T(1,128)S(1)}, u32[]{:S(2)}, u32[]{:S(2)}) collective-permute-start(f32[1,512]{1,0:T(1,128)S(1)} %get-tuple-element.35.refs_0_), channel_id=1, source_target_pairs={{0,1},{1,0},{2,3},{3,2},{4,5},{5,4},{6,7},{7,6},{8,9},{9,8},{10,11... | collective-permute-start | bytes 6152 | tf_op jit(solution)/shard_map/ppermute | solution.py:327
  (8 other events, 35.6 us)
where the time goes:
time: 118 us; the launch traced here: 116 us
  starting transfers between devices  47 us (40%)
  waiting for transfers between devices  42.9 us (36%)
  Pallas kernels  21.8 us (18%)
  local copies, waits for them, and re-layouts  3.92 us (3%)
    ppermute x12, starting transfers between devices, ring_gather(): lax.ppermute(chunks[sign * (step - 1)][half], axis, pairs)  37.1 us
    ppermute x12, waiting for transfers between devices, ring_gather(): lax.ppermute(chunks[sign * (step - 1)][half], axis, pairs)  30.1 us
    pallas_call x7, Pallas kernels, call(): pl.pallas_call(kernel, grid_spec=spec, out_shape=out_shape, compiler_para...  13.4 us
    ppermute x11, waiting for transfers between devices, swap(): return lax.ppermute(array, axis, [(i, i ^ bit) for i in range(size)])  8.03 us
    pallas_call x7, Pallas kernels, small(): pl.pallas_call(kernel, out_shape=tuple((pltpu.VMEM(*out) for out in outs)...  7.12 us
    ppermute x11, starting transfers between devices, swap(): return lax.ppermute(array, axis, [(i, i ^ bit) for i in range(size)])  5.16 us
    ppermute x1, waiting for transfers between devices, ring_gather(): lax.ppermute(chunks[last - 1][1], axis, backward)  4.67 us
    unnamed x24, local copies, waits for them, and re-layouts  3.92 us
  transfers between devices with their start and end apart: 28, of which 11 were waited for; matrix products, arithmetic and copies ran while one was open for 0% of the time, Pallas kernels for 16%

commit v1 on v0

--- a/solution.py
+++ b/solution.py
@@ -379,6 +379,9 @@
     branch_norm_gain,
     residual,
 ):
+    query_logits, forget_logits, value_inputs, output_gate_logits, surge_log_decay = (
+        outside(a) for a in (query_logits, forget_logits, value_inputs, output_gate_logits, surge_log_decay)
+    )
     rows, head_cols = query_logits.shape
     heads = head_cols // HEAD_DIM
     sp, tp = lax.axis_size("sp"), lax.axis_size("tp")
@@ -390,7 +393,7 @@
     ringed = is_ringed(sp, tp)
 
     group = heads // 2
-    per = 2
+    per = 4
     steps = group // per
     gap = forget_floor_gap.reshape(-1, 1, HEAD_DIM)
     block = pl.BlockSpec((rows, per * HEAD_DIM), lambda s, first, at: (0, first[0] + s))
@@ -399,11 +402,11 @@
     wide = jax.ShapeDtypeStruct((rows, group * HEAD_DIM), f32)
     narrow = jax.ShapeDtypeStruct((rows, group * HEAD_DIM), bf16)
 
-    def group_states(first, place=lambda array: array):
+    def group_states(first):
         return call(
             states_kernel,
             (first, tp_at),
-            [place(array) for array in (forget_logits, value_inputs, surge_log_decay, gap)],
+            (forget_logits, value_inputs, surge_log_decay, outside(gap)),
             (wide, pltpu.VMEM((group, HEAD_DIM + EXTRA, HEAD_DIM), bf16)),
             (steps,),
             [block, block, pl.BlockSpec((heads, rows), lambda s, first, at: (0, 0)), gap_block],
@@ -528,4 +531,7 @@
         P(),
         P("sp", "tp"),
     )
-    return jax.shard_map(layer, mesh=mesh, in_specs=placed, out_specs=P("sp", "tp"), check_vma=False)
+    step = jax.shard_map(layer, mesh=mesh, in_specs=placed, out_specs=P("sp", "tp"), check_vma=False)
+    if not is_ringed(mesh.shape["sp"], mesh.shape["tp"]):
+        return step
+    return step

time: 118 us -> 119 us (level)
  local copies, waits for them, and re-layouts: 3.92 us -> 0.02 us
  Pallas kernels: 21.8 us -> 25.3 us
    unnamed x24 -> x8, local copies, waits for them, and re-layouts: 3.92 us -> 0.02 us
    pallas_call x7, Pallas kernels: 13.4 us -> 16.9 us  [call(): pl.pallas_call(kernel, grid_spec=spec, out_shape=out_shape, compiler_para...]
    ppermute x11, waiting for transfers between devices: 8.03 us -> 10.7 us  [swap(): return lax.ppermute(array, axis, [(i, i ^ bit) for i in range(size)])]
    ppermute x12, waiting for transfers between devices: 30.1 us -> 28.3 us  [ring_gather(): lax.ppermute(chunks[sign * (step - 1)][half], axis, pairs)]
  transfers between devices with their start and end apart: 28 -> 28, of which waited for: 11 -> 12; matrix products, arithmetic and copies ran while one was open for 0% -> 0% of each run, Pallas kernels for 16% -> 19%
where the time goes in v1:
time: 119 us; the launch traced here: 116 us
  starting transfers between devices  47 us (39%)
  waiting for transfers between devices  43.8 us (37%)
  Pallas kernels  25.3 us (21%)
    ppermute x12, starting transfers between devices, ring_gather(): lax.ppermute(chunks[sign * (step - 1)][half], axis, pairs)  37.7 us
    ppermute x12, waiting for transfers between devices, ring_gather(): lax.ppermute(chunks[sign * (step - 1)][half], axis, pairs)  28.3 us
    pallas_call x7, Pallas kernels, call(): pl.pallas_call(kernel, grid_spec=spec, out_shape=out_shape, compiler_para...  16.9 us
    ppermute x11, waiting for transfers between devices, swap(): return lax.ppermute(array, axis, [(i, i ^ bit) for i in range(size)])  10.7 us
    pallas_call x7, Pallas kernels, small(): pl.pallas_call(kernel, out_shape=tuple((pltpu.VMEM(*out) for out in outs)...  7.14 us
    ppermute x11, starting transfers between devices, swap(): return lax.ppermute(array, axis, [(i, i ^ bit) for i in range(size)])  5.15 us
    ppermute x1, waiting for transfers between devices, ring_gather(): lax.ppermute(chunks[last - 1][1], axis, backward)  4.67 us
    ppermute x3, starting transfers between devices, carried_states(): before.append(lax.ppermute(sent, axis, pairs))  2.63 us
  transfers between devices with their start and end apart: 28, of which 12 were waited for; matrix products, arithmetic and copies ran while one was open for 0% of the time, Pallas kernels for 19%

profile of v1, /device:TPU:0, one launch (start us, length us, event | category | flops | bytes accessed | tf_op | source)
XLA Modules:
  0.0 116.4 jit_solution(13693636306970090052)
XLA Ops:
  0.0 1.2 %halves.1 = (bf16[256,1024]{1,0:T(8,128)(2,1)S(1)}, bf16[256,1024]{1,0:T(8,128)(2,1)S(1)}) custom-call(bf16[512,1024]{1,0:T(8,128)(2,1)} %matrix_ref.1), custom_call_target="tpu_custom_call" | custom-call | tf_op jit(solution)/shard_map/halves/pallas_call | solution.py:449
  1.2 3.1 %collective-permute-start.8 = (bf16[256,1024]{1,0:T(8,128)(2,1)S(1)}, bf16[256,1024]{1,0:T(8,128)(2,1)S(1)}, u32[]{:S(2)}, u32[]{:S(2)}) collective-permute-start(bf16[256,1024]{1,0:T(8,128)(2,1)S(1)} %get-tuple-element.27.refs_4_), channel_id=1, source_target_pairs={{0,8},{8,16},{16,24},{24,28},{28,20},{20,12},{12,4},{4,0},{1,9},{9... | collective-permute-start | bytes 1572872 | tf_op jit(solution)/shard_map/ppermute | solution.py:319
  4.3 2.9 %shard_map.100 = (f32[512,512]{1,0:T(8,128)S(1)}, bf16[4,136,128]{2,1,0:T(8,128)(2,1)S(1)}) custom-call(s32[1]{0:T(128)S(6)} %sub.3.first_ref, s32[1]{0:T(128)} %bitcast.tp_ref.at, bf16[512,1024]{1,0:T(8,128)(2,1)} %forget_ref.7, bf16[512,1024]{1,0:T(8,128)(2,1)} %value_ref.7, f32[8,512]{1,0:T(8,128)} %surge_ref.3, f32[32,1,128]{2,1,0:T(1,128)} %bitcast.5), custom_call_target="tpu_custom_call" | custom-call | tf_op jit(solution)/shard_map/pallas_call | solution.py:302
  7.3 2.9 %shard_map.102 = (f32[512,512]{1,0:T(8,128)S(1)}, bf16[4,136,128]{2,1,0:T(8,128)(2,1)S(1)}) custom-call(s32[1]{0:T(128)S(6)} %select_n.9.first_ref.odd_ref, s32[1]{0:T(128)} %bitcast.tp_ref.at, bf16[512,1024]{1,0:T(8,128)(2,1)} %forget_ref.7, bf16[512,1024]{1,0:T(8,128)(2,1)} %value_ref.7, f32[8,512]{1,0:T(8,128)} %surge_ref.3, f32[32,1,128]{2,1,0:T(1,128)} %bitcast.6), custom_call_target="tpu_custom_call" | custom-call | tf_op jit(solution)/shard_map/pallas_call | solution.py:302
  10.2 9.0 %collective-permute-done.other_ref.refs_4_ = bf16[4,136,128]{2,1,0:T(8,128)(2,1)S(1)} collective-permute-done((bf16[4,136,128]{2,1,0:T(8,128)(2,1)S(1)}, bf16[4,136,128]{2,1,0:T(8,128)(2,1)S(1)}, u32[]{:S(2)}, u32[]{:S(2)}) %collective-permute-start) | collective-permute-done | bytes 139296 | tf_op jit(solution)/shard_map/ppermute | solution.py:327
  19.2 1.3 %collective-permute-start.1 = (bf16[4,136,128]{2,1,0:T(8,128)(2,1)S(1)}, bf16[4,136,128]{2,1,0:T(8,128)(2,1)S(1)}, u32[]{:S(2)}, u32[]{:S(2)}) collective-permute-start(bf16[4,136,128]{2,1,0:T(8,128)(2,1)S(1)} %shard_map.103.refs_2_.refs_3_), channel_id=1, source_target_pairs={{0,8},{4,12},{1,9},{5,13},{2,10},{6,14},{3,11},{7,15}} | collective-permute-start | bytes 417800 | tf_op jit(solution)/shard_map/ppermute | solution.py:356
  20.6 2.0 %collective-permute-start.9 = (bf16[256,1024]{1,0:T(8,128)(2,1)S(1)}, bf16[256,1024]{1,0:T(8,128)(2,1)S(1)}, u32[]{:S(2)}, u32[]{:S(2)}) collective-permute-start(bf16[256,1024]{1,0:T(8,128)(2,1)S(1)} %get-tuple-element.28.refs_5_), channel_id=1, source_target_pairs={{0,8},{8,16},{16,24},{24,28},{28,20},{20,12},{12,4},{4,0},{1,9},{9... | collective-permute-start | bytes 1572872 | tf_op jit(solution)/shard_map/ppermute | solution.py:319
  22.7 2.0 %collective-permute-start.12 = (bf16[256,1024]{1,0:T(8,128)(2,1)S(1)}, bf16[256,1024]{1,0:T(8,128)(2,1)S(1)}, u32[]{:S(2)}, u32[]{:S(2)}) collective-permute-start(bf16[256,1024]{1,0:T(8,128)(2,1)S(1)} %collective-permute-done.8.refs_6_.refs_4_), channel_id=1, source_target_pairs={{0,8},{8,16},{16,24},{24,28},{28,20},{20,12},{12,4},{4,0},{1,9},{9... | collective-permute-start | bytes 1572872 | tf_op jit(solution)/shard_map/ppermute | solution.py:319
  26.5 3.1 %shard_map.108 = (f32[512,512]{1,0:T(8,128)S(1)}, bf16[512,512]{1,0:T(8,128)(2,1)S(1)}) custom-call(s32[1]{0:T(128)S(6)} %select_n.9.first_ref.odd_ref, s32[1]{0:T(128)} %bitcast.tp_ref.at, bf16[512,1024]{1,0:T(8,128)(2,1)} %query_ref.3, bf16[512,1024]{1,0:T(8,128)(2,1)} %forget_ref.7, bf16[512,1024]{1,0:T(8,128)(2,1)} %value_ref.7, ...), custom_call_target="tpu_custom_call" | custom-call | tf_op jit(solution)/shard_map/pallas_call | solution.py:302
  29.6 5.7 %collective-permute-done.11.refs_9_.refs_7_ = bf16[256,1024]{1,0:T(8,128)(2,1)S(1)} collective-permute-done((bf16[256,1024]{1,0:T(8,128)(2,1)S(1)}, bf16[256,1024]{1,0:T(8,128)(2,1)S(1)}, u32[]{:S(2)}, u32[]{:S(2)}) %collective-permute-start.11) | collective-permute-done | bytes 524320 | tf_op jit(solution)/shard_map/ppermute | solution.py:319
  35.8 16.0 %collective-permute-start.13 = (bf16[256,1024]{1,0:T(8,128)(2,1)S(1)}, bf16[256,1024]{1,0:T(8,128)(2,1)S(1)}, u32[]{:S(2)}, u32[]{:S(2)}) collective-permute-start(bf16[256,1024]{1,0:T(8,128)(2,1)S(1)} %collective-permute-done.9.refs_7_.refs_5_), channel_id=1, source_target_pairs={{0,8},{8,16},{16,24},{24,28},{28,20},{20,12},{12,4},{4,0},{1,9},{9... | collective-permute-start | bytes 1572872 | tf_op jit(solution)/shard_map/ppermute | solution.py:319
  51.8 2.0 %collective-permute-start.14 = (bf16[256,1024]{1,0:T(8,128)(2,1)S(1)}, bf16[256,1024]{1,0:T(8,128)(2,1)S(1)}, u32[]{:S(2)}, u32[]{:S(2)}) collective-permute-start(bf16[256,1024]{1,0:T(8,128)(2,1)S(1)} %collective-permute-done.10.refs_8_.refs_6_), channel_id=1, source_target_pairs={{8,0},{16,8},{24,16},{28,24},{20,28},{12,20},{4,12},{0,4},{9,1},{1... | collective-permute-start | bytes 1572872 | tf_op jit(solution)/shard_map/ppermute | solution.py:319
  53.8 1.8 %shard_map.109.refs_0_ = bf16[512,512]{1,0:T(8,128)(2,1)S(1)} custom-call(s32[1]{0:T(128)S(6)} %select_n.9.first_ref.odd_ref, f32[512,512]{1,0:T(8,128)S(1)} %get-tuple-element.30.local_ref, bf16[512,512]{1,0:T(8,128)(2,1)S(1)} %get-tuple-element.31.reach_ref, bf16[4,128,128]{2,1,0:T(8,128)(2,1)S(1)} %get-tuple-element.32.carried_ref, ...), custom_call_target="tpu_custom_call" | custom-call | tf_op jit(solution)/shard_map/pallas_call | solution.py:302
  55.6 1.6 %collective-permute-start.21 = (bf16[512,512]{1,0:T(8,128)(2,1)S(1)}, bf16[512,512]{1,0:T(8,128)(2,1)S(1)}, u32[]{:S(2)}, u32[]{:S(2)}) collective-permute-start(bf16[512,512]{1,0:T(8,128)(2,1)S(1)} %shard_map.109.refs_0_), channel_id=1, source_target_pairs={{0,2},{1,3},{2,0},{3,1},{4,6},{5,7},{6,4},{7,5},{8,10},{9,11},{10,... | collective-permute-start | bytes 1572872 | tf_op jit(solution)/shard_map/ppermute | solution.py:327
  57.1 3.1 %shard_map.101 = (f32[512,512]{1,0:T(8,128)S(1)}, bf16[512,512]{1,0:T(8,128)(2,1)S(1)}) custom-call(s32[1]{0:T(128)S(6)} %sub.3.first_ref, s32[1]{0:T(128)} %bitcast.tp_ref.at, bf16[512,1024]{1,0:T(8,128)(2,1)} %query_ref.3, bf16[512,1024]{1,0:T(8,128)(2,1)} %forget_ref.7, bf16[512,1024]{1,0:T(8,128)(2,1)} %value_ref.7, ...), custom_call_target="tpu_custom_call" | custom-call | tf_op jit(solution)/shard_map/pallas_call | solution.py:302
  60.2 1.8 %shard_map.107.refs_0_ = bf16[512,512]{1,0:T(8,128)(2,1)S(1)} custom-call(s32[1]{0:T(128)S(6)} %sub.3.first_ref, f32[512,512]{1,0:T(8,128)S(1)} %get-tuple-element.22.local_ref, bf16[512,512]{1,0:T(8,128)(2,1)S(1)} %get-tuple-element.23.reach_ref, bf16[4,128,128]{2,1,0:T(8,128)(2,1)S(1)} %collective-permute-done.4.carried_ref, bf16[512,1024]{1,0:T(8,128)(2,1)} %gate_ref.3, ...), custom_call_target="tpu_custom_call" | custom-call | tf_op jit(solution)/shard_map/pallas_call | solution.py:302
  62.0 2.4 %collective-permute-done.15.refs_13_.refs_11_ = bf16[256,1024]{1,0:T(8,128)(2,1)S(1)} collective-permute-done((bf16[256,1024]{1,0:T(8,128)(2,1)S(1)}, bf16[256,1024]{1,0:T(8,128)(2,1)S(1)}, u32[]{:S(2)}, u32[]{:S(2)}) %collective-permute-start.15) | collective-permute-done | bytes 524320 | tf_op jit(solution)/shard_map/ppermute | solution.py:319
  64.5 1.5 %collective-permute-start.6 = (bf16[512,512]{1,0:T(8,128)(2,1)S(1)}, bf16[512,512]{1,0:T(8,128)(2,1)S(1)}, u32[]{:S(2)}, u32[]{:S(2)}) collective-permute-start(bf16[512,512]{1,0:T(8,128)(2,1)S(1)} %shard_map.107.refs_0_), channel_id=1, source_target_pairs={{0,2},{1,3},{2,0},{3,1},{4,6},{5,7},{6,4},{7,5},{8,10},{9,11},{10,... | collective-permute-start | bytes 1572872 | tf_op jit(solution)/shard_map/ppermute | solution.py:327
  66.0 5.7 %collective-permute-start.16 = (bf16[256,1024]{1,0:T(8,128)(2,1)S(1)}, bf16[256,1024]{1,0:T(8,128)(2,1)S(1)}, u32[]{:S(2)}, u32[]{:S(2)}) collective-permute-start(bf16[256,1024]{1,0:T(8,128)(2,1)S(1)} %collective-permute-done.12.refs_10_.refs_8_), channel_id=1, source_target_pairs={{0,8},{8,16},{16,24},{24,28},{28,20},{20,12},{12,4},{4,0},{1,9},{9... | collective-permute-start | bytes 1572872 | tf_op jit(solution)/shard_map/ppermute | solution.py:319
  71.6 1.8 %collective-permute-done.14.refs_12_.refs_10_ = bf16[256,1024]{1,0:T(8,128)(2,1)S(1)} collective-permute-done((bf16[256,1024]{1,0:T(8,128)(2,1)S(1)}, bf16[256,1024]{1,0:T(8,128)(2,1)S(1)}, u32[]{:S(2)}, u32[]{:S(2)}) %collective-permute-start.14) | collective-permute-done | bytes 524320 | tf_op jit(solution)/shard_map/ppermute | solution.py:319
  74.4 4.1 %collective-permute-start.17 = (bf16[256,1024]{1,0:T(8,128)(2,1)S(1)}, bf16[256,1024]{1,0:T(8,128)(2,1)S(1)}, u32[]{:S(2)}, u32[]{:S(2)}) collective-permute-start(bf16[256,1024]{1,0:T(8,128)(2,1)S(1)} %collective-permute-done.13.refs_11_.refs_9_), channel_id=1, source_target_pairs={{0,8},{8,16},{16,24},{24,28},{28,20},{20,12},{12,4},{4,0},{1,9},{9... | collective-permute-start | bytes 1572872 | tf_op jit(solution)/shard_map/ppermute | solution.py:319
  78.5 1.7 %collective-permute-start.18 = (bf16[256,1024]{1,0:T(8,128)(2,1)S(1)}, bf16[256,1024]{1,0:T(8,128)(2,1)S(1)}, u32[]{:S(2)}, u32[]{:S(2)}) collective-permute-start(bf16[256,1024]{1,0:T(8,128)(2,1)S(1)} %collective-permute-done.14.refs_12_.refs_10_), channel_id=1, source_target_pairs={{8,0},{16,8},{24,16},{28,24},{20,28},{12,20},{4,12},{0,4},{9,1},{1... | collective-permute-start | bytes 1572872 | tf_op jit(solution)/shard_map/ppermute | solution.py:319
  80.3 1.2 %collective-permute-done.16.refs_14_.refs_12_ = bf16[256,1024]{1,0:T(8,128)(2,1)S(1)} collective-permute-done((bf16[256,1024]{1,0:T(8,128)(2,1)S(1)}, bf16[256,1024]{1,0:T(8,128)(2,1)S(1)}, u32[]{:S(2)}, u32[]{:S(2)}) %collective-permute-start.16) | collective-permute-done | bytes 524320 | tf_op jit(solution)/shard_map/ppermute | solution.py:319
  81.5 9.8 %collective-permute-done.19.refs_17_.refs_15_ = bf16[256,1024]{1,0:T(8,128)(2,1)S(1)} collective-permute-done((bf16[256,1024]{1,0:T(8,128)(2,1)S(1)}, bf16[256,1024]{1,0:T(8,128)(2,1)S(1)}, u32[]{:S(2)}, u32[]{:S(2)}) %collective-permute-start.19) | collective-permute-done | bytes 524320 | tf_op jit(solution)/shard_map/ppermute | solution.py:319
  91.9 1.6 %collective-permute-start.23 = (bf16[256,1024]{1,0:T(8,128)(2,1)S(1)}, bf16[256,1024]{1,0:T(8,128)(2,1)S(1)}, u32[]{:S(2)}, u32[]{:S(2)}) collective-permute-start(bf16[256,1024]{1,0:T(8,128)(2,1)S(1)} %collective-permute-done.16.refs_14_.refs_12_), channel_id=1, source_target_pairs={{0,8},{8,16},{16,24},{24,28},{28,20},{20,12},{12,4},{4,0},{1,9},{9... | collective-permute-start | bytes 1572872 | tf_op jit(solution)/shard_map/ppermute | solution.py:321
  93.5 6.4 %collective-permute-done.18.refs_16_.refs_14_ = bf16[256,1024]{1,0:T(8,128)(2,1)S(1)} collective-permute-done((bf16[256,1024]{1,0:T(8,128)(2,1)S(1)}, bf16[256,1024]{1,0:T(8,128)(2,1)S(1)}, u32[]{:S(2)}, u32[]{:S(2)}) %collective-permute-start.18) | collective-permute-done | bytes 524320 | tf_op jit(solution)/shard_map/ppermute | solution.py:319
  99.8 3.2 %shard_map.110.refs_16_ = f32[512,1024]{1,0:T(8,128)S(1)} custom-call(s32[1]{0:T(128)} %bitcast.1.refs_0_.at_ref.sp_ref, s32[1]{0:T(128)} %bitcast.tp_ref.at, bf16[512,512]{1,0:T(8,128)(2,1)S(1)} %shard_map.109.refs_0_, bf16[512,512]{1,0:T(8,128)(2,1)S(1)} %collective-permute-done.20.refs_1_, bf16[512,512]{1,0:T(8,128)(2,1)S(1)} %collective-permute-done.21.refs_2_, ...), custom_call_target="tpu_custom_call" | custom-call | tf_op jit(solution)/shard_map/pallas_call | solution.py:284
  103.1 2.5 %shard_map.111 = (f32[512,1024]{1,0:T(8,128)S(1)}, bf16[512,512]{1,0:T(8,128)(2,1)S(1)}) custom-call(s32[1]{0:T(128)} %bitcast.1.refs_0_.at_ref.sp_ref, s32[1]{0:T(128)} %bitcast.tp_ref.at, bf16[512,512]{1,0:T(8,128)(2,1)S(1)} %shard_map.107.refs_0_, bf16[512,512]{1,0:T(8,128)(2,1)S(1)} %collective-permute-done.5.refs_1_, ...), custom_call_target="tpu_custom_call" | custom-call | tf_op jit(solution)/shard_map/pallas_call | solution.py:284
  105.6 4.7 %collective-permute-done.24.second_ref = bf16[256,1024]{1,0:T(8,128)(2,1)S(1)} collective-permute-done((bf16[256,1024]{1,0:T(8,128)(2,1)S(1)}, bf16[256,1024]{1,0:T(8,128)(2,1)S(1)}, u32[]{:S(2)}, u32[]{:S(2)}) %collective-permute-start.24) | collective-permute-done | bytes 524320 | tf_op jit(solution)/shard_map/ppermute | solution.py:321
  111.3 1.0 collective-permute-start.26
  113.2 1.1 collective-permute-done.25.refs_1_
  114.9 1.3 %shard_map.113 = bf16[512,1024]{1,0:T(8,128)(2,1)} custom-call(s32[1]{0:T(128)} %bitcast.tp_ref.at, f32[1,512]{1,0:T(1,128)S(1)} %get-tuple-element.35.refs_0_, f32[1,512]{1,0:T(1,128)S(1)} %collective-permute-done.25.refs_1_, f32[1,512]{1,0:T(1,128)S(1)} %collective-permute-done.26.refs_2_, f32[1,512]{1,0:T(1,128)S(1)} %collective-permute-done.27.refs_3_, ...), custom_call_target="tpu_custom_call" | custom-call | tf_op jit(solution)/shard_map/pallas_call | solution.py:302
  (47 shorter events, 6.6 us)
Async XLA Ops:
  1.2 21.5 %collective-permute-start.8 = (bf16[256,1024]{1,0:T(8,128)(2,1)S(1)}, bf16[256,1024]{1,0:T(8,128)(2,1)S(1)}, u32[]{:S(2)}, u32[]{:S(2)}) collective-permute-start(bf16[256,1024]{1,0:T(8,128)(2,1)S(1)} %get-tuple-element.27.refs_4_), channel_id=1, source_target_pairs={{0,8},{8,16},{16,24},{24,28},{28,20},{20,12},{12,4},{4,0},{1,9},{9... | collective-permute-start | bytes 1572872 | tf_op jit(solution)/shard_map/ppermute | solution.py:319
  7.2 19.3 %copy-start.1 = (f32[4096]{0:T(1024)S(1)}, f32[4096]{0:T(1024)}, u32[]{:S(2)}) copy-start(f32[4096]{0:T(1024)} %param.14) | copy-start | bytes 49156
  7.2 11.9 %collective-permute-start = (bf16[4,136,128]{2,1,0:T(8,128)(2,1)S(1)}, bf16[4,136,128]{2,1,0:T(8,128)(2,1)S(1)}, u32[]{:S(2)}, u32[]{:S(2)}) collective-permute-start(bf16[4,136,128]{2,1,0:T(8,128)(2,1)S(1)} %get-tuple-element.25), channel_id=1, source_target_pairs={{0,4},{4,0},{8,12},{12,8},{16,20},{20,16},{24,28},{28,24},{1,5},{5... | collective-permute-start | bytes 417800 | tf_op jit(solution)/shard_map/ppermute | solution.py:327
  19.2 5.4 %collective-permute-start.1 = (bf16[4,136,128]{2,1,0:T(8,128)(2,1)S(1)}, bf16[4,136,128]{2,1,0:T(8,128)(2,1)S(1)}, u32[]{:S(2)}, u32[]{:S(2)}) collective-permute-start(bf16[4,136,128]{2,1,0:T(8,128)(2,1)S(1)} %shard_map.103.refs_2_.refs_3_), channel_id=1, source_target_pairs={{0,8},{4,12},{1,9},{5,13},{2,10},{6,14},{3,11},{7,15}} | collective-permute-start | bytes 417800 | tf_op jit(solution)/shard_map/ppermute | solution.py:356
  20.5 14.8 %collective-permute-start.11 = (bf16[256,1024]{1,0:T(8,128)(2,1)S(1)}, bf16[256,1024]{1,0:T(8,128)(2,1)S(1)}, u32[]{:S(2)}, u32[]{:S(2)}) collective-permute-start(bf16[256,1024]{1,0:T(8,128)(2,1)S(1)} %get-tuple-element.28.refs_5_), channel_id=1, source_target_pairs={{8,0},{16,8},{24,16},{28,24},{20,28},{12,20},{4,12},{0,4},{9,1},{1... | collective-permute-start | bytes 1572872 | tf_op jit(solution)/shard_map/ppermute | solution.py:319
  20.6 15.2 %collective-permute-start.9 = (bf16[256,1024]{1,0:T(8,128)(2,1)S(1)}, bf16[256,1024]{1,0:T(8,128)(2,1)S(1)}, u32[]{:S(2)}, u32[]{:S(2)}) collective-permute-start(bf16[256,1024]{1,0:T(8,128)(2,1)S(1)} %get-tuple-element.28.refs_5_), channel_id=1, source_target_pairs={{0,8},{8,16},{16,24},{24,28},{28,20},{20,12},{12,4},{4,0},{1,9},{9... | collective-permute-start | bytes 1572872 | tf_op jit(solution)/shard_map/ppermute | solution.py:319
  22.6 29.2 %collective-permute-start.10 = (bf16[256,1024]{1,0:T(8,128)(2,1)S(1)}, bf16[256,1024]{1,0:T(8,128)(2,1)S(1)}, u32[]{:S(2)}, u32[]{:S(2)}) collective-permute-start(bf16[256,1024]{1,0:T(8,128)(2,1)S(1)} %get-tuple-element.27.refs_4_), channel_id=1, source_target_pairs={{8,0},{16,8},{24,16},{28,24},{20,28},{12,20},{4,12},{0,4},{9,1},{1... | collective-permute-start | bytes 1572872 | tf_op jit(solution)/shard_map/ppermute | solution.py:319
  22.7 34.4 %collective-permute-start.12 = (bf16[256,1024]{1,0:T(8,128)(2,1)S(1)}, bf16[256,1024]{1,0:T(8,128)(2,1)S(1)}, u32[]{:S(2)}, u32[]{:S(2)}) collective-permute-start(bf16[256,1024]{1,0:T(8,128)(2,1)S(1)} %collective-permute-done.8.refs_6_.refs_4_), channel_id=1, source_target_pairs={{0,8},{8,16},{16,24},{24,28},{28,20},{20,12},{12,4},{4,0},{1,9},{9... | collective-permute-start | bytes 1572872 | tf_op jit(solution)/shard_map/ppermute | solution.py:319
  24.7 0.7 collective-permute-start.2
  25.5 0.7 collective-permute-start.3
  26.4 29.2 %collective-permute-start.4 = (bf16[4,128,128]{2,1,0:T(8,128)(2,1)S(1)}, bf16[4,128,128]{2,1,0:T(8,128)(2,1)S(1)}, u32[]{:S(2)}, u32[]{:S(2)}) collective-permute-start(bf16[4,128,128]{2,1,0:T(8,128)(2,1)S(1)} %get-tuple-element.26), channel_id=1, source_target_pairs={{0,4},{4,0},{8,12},{12,8},{16,20},{20,16},{24,28},{28,24},{1,5},{5... | collective-permute-start | bytes 393224 | tf_op jit(solution)/shard_map/ppermute | solution.py:327
  26.5 27.2 %copy-start.3 = (f32[128]{0:T(128)S(1)}, f32[128]{0:T(128)}, u32[]{:S(2)}) copy-start(f32[128]{0:T(128)} %param.16) | copy-start | bytes 1540
  35.4 29.1 %collective-permute-start.15 = (bf16[256,1024]{1,0:T(8,128)(2,1)S(1)}, bf16[256,1024]{1,0:T(8,128)(2,1)S(1)}, u32[]{:S(2)}, u32[]{:S(2)}) collective-permute-start(bf16[256,1024]{1,0:T(8,128)(2,1)S(1)} %collective-permute-done.11.refs_9_.refs_7_), channel_id=1, source_target_pairs={{8,0},{16,8},{24,16},{28,24},{20,28},{12,20},{4,12},{0,4},{9,1},{1... | collective-permute-start | bytes 1572872 | tf_op jit(solution)/shard_map/ppermute | solution.py:319
  35.8 30.2 %collective-permute-start.13 = (bf16[256,1024]{1,0:T(8,128)(2,1)S(1)}, bf16[256,1024]{1,0:T(8,128)(2,1)S(1)}, u32[]{:S(2)}, u32[]{:S(2)}) collective-permute-start(bf16[256,1024]{1,0:T(8,128)(2,1)S(1)} %collective-permute-done.9.refs_7_.refs_5_), channel_id=1, source_target_pairs={{0,8},{8,16},{16,24},{24,28},{28,20},{20,12},{12,4},{4,0},{1,9},{9... | collective-permute-start | bytes 1572872 | tf_op jit(solution)/shard_map/ppermute | solution.py:319
  51.8 21.6 %collective-permute-start.14 = (bf16[256,1024]{1,0:T(8,128)(2,1)S(1)}, bf16[256,1024]{1,0:T(8,128)(2,1)S(1)}, u32[]{:S(2)}, u32[]{:S(2)}) collective-permute-start(bf16[256,1024]{1,0:T(8,128)(2,1)S(1)} %collective-permute-done.10.refs_8_.refs_6_), channel_id=1, source_target_pairs={{8,0},{16,8},{24,16},{28,24},{20,28},{12,20},{4,12},{0,4},{9,1},{1... | collective-permute-start | bytes 1572872 | tf_op jit(solution)/shard_map/ppermute | solution.py:319
  55.6 18.8 %collective-permute-start.21 = (bf16[512,512]{1,0:T(8,128)(2,1)S(1)}, bf16[512,512]{1,0:T(8,128)(2,1)S(1)}, u32[]{:S(2)}, u32[]{:S(2)}) collective-permute-start(bf16[512,512]{1,0:T(8,128)(2,1)S(1)} %shard_map.109.refs_0_), channel_id=1, source_target_pairs={{0,2},{1,3},{2,0},{3,1},{4,6},{5,7},{6,4},{7,5},{8,10},{9,11},{10,... | collective-permute-start | bytes 1572872 | tf_op jit(solution)/shard_map/ppermute | solution.py:327
  57.1 21.4 %collective-permute-start.20 = (bf16[512,512]{1,0:T(8,128)(2,1)S(1)}, bf16[512,512]{1,0:T(8,128)(2,1)S(1)}, u32[]{:S(2)}, u32[]{:S(2)}) collective-permute-start(bf16[512,512]{1,0:T(8,128)(2,1)S(1)} %shard_map.109.refs_0_), channel_id=1, source_target_pairs={{0,1},{1,0},{2,3},{3,2},{4,5},{5,4},{6,7},{7,6},{8,9},{9,8},{10,11... | collective-permute-start | bytes 1572872 | tf_op jit(solution)/shard_map/ppermute | solution.py:327
  64.5 15.8 %collective-permute-start.6 = (bf16[512,512]{1,0:T(8,128)(2,1)S(1)}, bf16[512,512]{1,0:T(8,128)(2,1)S(1)}, u32[]{:S(2)}, u32[]{:S(2)}) collective-permute-start(bf16[512,512]{1,0:T(8,128)(2,1)S(1)} %shard_map.107.refs_0_), channel_id=1, source_target_pairs={{0,2},{1,3},{2,0},{3,1},{4,6},{5,7},{6,4},{7,5},{8,10},{9,11},{10,... | collective-permute-start | bytes 1572872 | tf_op jit(solution)/shard_map/ppermute | solution.py:327
  66.0 15.5 %collective-permute-start.16 = (bf16[256,1024]{1,0:T(8,128)(2,1)S(1)}, bf16[256,1024]{1,0:T(8,128)(2,1)S(1)}, u32[]{:S(2)}, u32[]{:S(2)}) collective-permute-start(bf16[256,1024]{1,0:T(8,128)(2,1)S(1)} %collective-permute-done.12.refs_10_.refs_8_), channel_id=1, source_target_pairs={{0,8},{8,16},{16,24},{24,28},{28,20},{20,12},{12,4},{4,0},{1,9},{9... | collective-permute-start | bytes 1572872 | tf_op jit(solution)/shard_map/ppermute | solution.py:319
  73.4 17.9 %collective-permute-start.19 = (bf16[256,1024]{1,0:T(8,128)(2,1)S(1)}, bf16[256,1024]{1,0:T(8,128)(2,1)S(1)}, u32[]{:S(2)}, u32[]{:S(2)}) collective-permute-start(bf16[256,1024]{1,0:T(8,128)(2,1)S(1)} %collective-permute-done.15.refs_13_.refs_11_), channel_id=1, source_target_pairs={{8,0},{16,8},{24,16},{28,24},{20,28},{12,20},{4,12},{0,4},{9,1},{1... | collective-permute-start | bytes 1572872 | tf_op jit(solution)/shard_map/ppermute | solution.py:319
  74.4 17.5 %collective-permute-start.17 = (bf16[256,1024]{1,0:T(8,128)(2,1)S(1)}, bf16[256,1024]{1,0:T(8,128)(2,1)S(1)}, u32[]{:S(2)}, u32[]{:S(2)}) collective-permute-start(bf16[256,1024]{1,0:T(8,128)(2,1)S(1)} %collective-permute-done.13.refs_11_.refs_9_), channel_id=1, source_target_pairs={{0,8},{8,16},{16,24},{24,28},{28,20},{20,12},{12,4},{4,0},{1,9},{9... | collective-permute-start | bytes 1572872 | tf_op jit(solution)/shard_map/ppermute | solution.py:319
  78.5 21.3 %collective-permute-start.18 = (bf16[256,1024]{1,0:T(8,128)(2,1)S(1)}, bf16[256,1024]{1,0:T(8,128)(2,1)S(1)}, u32[]{:S(2)}, u32[]{:S(2)}) collective-permute-start(bf16[256,1024]{1,0:T(8,128)(2,1)S(1)} %collective-permute-done.14.refs_12_.refs_10_), channel_id=1, source_target_pairs={{8,0},{16,8},{24,16},{28,24},{20,28},{12,20},{4,12},{0,4},{9,1},{1... | collective-permute-start | bytes 1572872 | tf_op jit(solution)/shard_map/ppermute | solution.py:319
  80.3 22.8 %collective-permute-start.5 = (bf16[512,512]{1,0:T(8,128)(2,1)S(1)}, bf16[512,512]{1,0:T(8,128)(2,1)S(1)}, u32[]{:S(2)}, u32[]{:S(2)}) collective-permute-start(bf16[512,512]{1,0:T(8,128)(2,1)S(1)} %shard_map.107.refs_0_), channel_id=1, source_target_pairs={{0,1},{1,0},{2,3},{3,2},{4,5},{5,4},{6,7},{7,6},{8,9},{9,8},{10,11... | collective-permute-start | bytes 1572872 | tf_op jit(solution)/shard_map/ppermute | solution.py:327
  81.5 18.3 %collective-permute-start.22 = (bf16[512,512]{1,0:T(8,128)(2,1)S(1)}, bf16[512,512]{1,0:T(8,128)(2,1)S(1)}, u32[]{:S(2)}, u32[]{:S(2)}) collective-permute-start(bf16[512,512]{1,0:T(8,128)(2,1)S(1)} %collective-permute-done.21.refs_2_), channel_id=1, source_target_pairs={{0,1},{1,0},{2,3},{3,2},{4,5},{5,4},{6,7},{7,6},{8,9},{9,8},{10,11... | collective-permute-start | bytes 1572872 | tf_op jit(solution)/shard_map/ppermute | solution.py:327
  91.3 11.8 %collective-permute-start.7 = (bf16[512,512]{1,0:T(8,128)(2,1)S(1)}, bf16[512,512]{1,0:T(8,128)(2,1)S(1)}, u32[]{:S(2)}, u32[]{:S(2)}) collective-permute-start(bf16[512,512]{1,0:T(8,128)(2,1)S(1)} %collective-permute-done.6.refs_2_), channel_id=1, source_target_pairs={{0,1},{1,0},{2,3},{3,2},{4,5},{5,4},{6,7},{7,6},{8,9},{9,8},{10,11... | collective-permute-start | bytes 1572872 | tf_op jit(solution)/shard_map/ppermute | solution.py:327
  91.9 13.8 %collective-permute-start.23 = (bf16[256,1024]{1,0:T(8,128)(2,1)S(1)}, bf16[256,1024]{1,0:T(8,128)(2,1)S(1)}, u32[]{:S(2)}, u32[]{:S(2)}) collective-permute-start(bf16[256,1024]{1,0:T(8,128)(2,1)S(1)} %collective-permute-done.16.refs_14_.refs_12_), channel_id=1, source_target_pairs={{0,8},{8,16},{16,24},{24,28},{28,20},{20,12},{12,4},{4,0},{1,9},{9... | collective-permute-start | bytes 1572872 | tf_op jit(solution)/shard_map/ppermute | solution.py:321
  99.8 10.5 %collective-permute-start.24 = (bf16[256,1024]{1,0:T(8,128)(2,1)S(1)}, bf16[256,1024]{1,0:T(8,128)(2,1)S(1)}, u32[]{:S(2)}, u32[]{:S(2)}) collective-permute-start(bf16[256,1024]{1,0:T(8,128)(2,1)S(1)} %collective-permute-done.19.refs_17_.refs_15_), channel_id=1, source_target_pairs={{8,0},{16,8},{24,16},{28,24},{20,28},{12,20},{4,12},{0,4},{9,1},{1... | collective-permute-start | bytes 1572872 | tf_op jit(solution)/shard_map/ppermute | solution.py:321
  105.6 9.3 %copy-start = (bf16[512,1024]{1,0:T(8,128)(2,1)S(1)}, bf16[512,1024]{1,0:T(8,128)(2,1)}, u32[]{:S(2)}) copy-start(bf16[512,1024]{1,0:T(8,128)(2,1)} %refs_5_.1) | copy-start | bytes 3145732
  105.6 9.3 %copy-start.2 = (f32[4096]{0:T(1024)S(1)}, f32[4096]{0:T(1024)}, u32[]{:S(2)}) copy-start(f32[4096]{0:T(1024)} %param.18) | copy-start | bytes 49156
  111.3 3.0 %collective-permute-start.25 = (f32[1,512]{1,0:T(1,128)S(1)}, f32[1,512]{1,0:T(1,128)S(1)}, u32[]{:S(2)}, u32[]{:S(2)}) collective-permute-start(f32[1,512]{1,0:T(1,128)S(1)} %get-tuple-element.35.refs_0_), channel_id=1, source_target_pairs={{0,3},{1,2},{2,1},{3,0},{4,7},{5,6},{6,5},{7,4},{8,11},{9,10},{10,... | collective-permute-start | bytes 6152 | tf_op jit(solution)/shard_map/ppermute | solution.py:327
  111.3 3.6 %collective-permute-start.26 = (f32[1,512]{1,0:T(1,128)S(1)}, f32[1,512]{1,0:T(1,128)S(1)}, u32[]{:S(2)}, u32[]{:S(2)}) collective-permute-start(f32[1,512]{1,0:T(1,128)S(1)} %get-tuple-element.35.refs_0_), channel_id=1, source_target_pairs={{0,2},{1,3},{2,0},{3,1},{4,6},{5,7},{6,4},{7,5},{8,10},{9,11},{10,... | collective-permute-start | bytes 6152 | tf_op jit(solution)/shard_map/ppermute | solution.py:327
  112.3 2.6 %collective-permute-start.27 = (f32[1,512]{1,0:T(1,128)S(1)}, f32[1,512]{1,0:T(1,128)S(1)}, u32[]{:S(2)}, u32[]{:S(2)}) collective-permute-start(f32[1,512]{1,0:T(1,128)S(1)} %get-tuple-element.35.refs_0_), channel_id=1, source_target_pairs={{0,1},{1,0},{2,3},{3,2},{4,5},{5,4},{6,7},{7,6},{8,9},{9,8},{10,11... | collective-permute-start | bytes 6152 | tf_op jit(solution)/shard_map/ppermute | solution.py:327
